TPU v7x, 768 devices: a whole 4x8x12 slice. The times are simulated.
768 devices in a mesh: ep: 48 (over z, x), tp: 16 (over y, core).
Axes of the slice: x: 4, y: 8, z: 12, core: 2. Of those that a mesh axis runs over, the one named last changes fastest.
Arguments:
- tokens: bfloat16 [147456, 2048], P(('ep', 'tp')), may hold values from -6 to 6
- routes: int32 [147456, 2], P(('ep', 'tp')), may hold values from 0 to 47, all different within a row; in each aligned block of 192 rows (0 to 191, 192 to 383, ...) at most 10 rows name the same one
- gates: float32 [147456, 2], P(('ep', 'tp')), may hold values from 0.3 to 2.2
- pre_gain: float32 [2048], replicated, may hold values from 0.1 to 1.9
- w_gate: bfloat16 [48, 2048, 512], P('ep'), may hold values from -0.125 to 0.125
- w_up: bfloat16 [48, 2048, 512], P('ep'), may hold values from -0.125 to 0.125
- w_down: bfloat16 [48, 512, 2048], P('ep'), may hold values from -0.25 to 0.25
- sh_gate: bfloat16 [2048, 512], P('tp'), may hold values from -0.125 to 0.125
- sh_up: bfloat16 [2048, 512], P('tp'), may hold values from -0.125 to 0.125
- sh_down: bfloat16 [512, 2048], P(None, 'tp'), may hold values from -0.25 to 0.25
- post_gain: float32 [2048], replicated, may hold values from 0.1 to 1.9
Outputs:
- mixed: bfloat16 [147456, 2048], P('ep', 'tp')
Inputs may be any that keep to these rules, and one draw needn't show every extreme that they name: `routes`: each token names 2 different experts; among the rows of one device no expert is named more than 10 times, a bound that some block reaches.
All inputs are finite; a program needn't handle non-finite values.
Results may differ from a plain program's by a relative error of at most 0.0075.
Values may be sent and summed in bfloat16 or wider, within the bound.
A program may use at most 64 MiB of HBM per device.

v0:
```python
import jax
import jax.numpy as jnp
from jax import lax
from jax.sharding import PartitionSpec as P

TOPK = 2


def per_device(
    tokens, routes, gates, pre_gain, w_gate, w_up, w_down, sh_gate, sh_up, sh_down, post_gain
):
    tok_rows, full_width = tokens.shape
    experts_all = lax.axis_size("ep")
    capacity = max(2, 4 * tok_rows * TOPK // (3 * experts_all))
    inputs = tokens.astype(jnp.float32)
    scale_in = lax.rsqrt(jnp.mean(inputs * inputs, axis=1, keepdims=True) + 1e-06)
    normed = (inputs * scale_in * pre_gain[None, :]).astype(jnp.bfloat16)
    gate_shared = jnp.dot(
        normed,
        lax.all_gather(sh_gate, "tp", axis=0, tiled=True),
        preferred_element_type=jnp.float32,
    )
    up_shared = jnp.dot(
        normed, lax.all_gather(sh_up, "tp", axis=0, tiled=True), preferred_element_type=jnp.float32
    )
    shared_hidden = (jax.nn.silu(gate_shared) * up_shared).astype(jnp.bfloat16)
    pair_count = tok_rows * TOPK
    expert_ids = routes.reshape(pair_count)
    matches = (expert_ids[:, None] == jnp.arange(experts_all, dtype=jnp.int32)[None, :]).astype(
        jnp.int32
    )
    earlier = jnp.cumsum(matches, axis=0) - matches
    slot_index = jnp.sum(earlier * matches, axis=1)
    dest_slot = expert_ids * capacity + slot_index
    pair_token = jnp.arange(pair_count, dtype=jnp.int32) // TOPK
    slot_token = (
        jnp.full((experts_all * capacity,), tok_rows, jnp.int32).at[dest_slot].set(pair_token)
    )
    padded = jnp.concatenate([normed, jnp.zeros((1, full_width), jnp.bfloat16)], axis=0)
    outgoing = padded[slot_token].reshape(experts_all, capacity, full_width)
    arrived = lax.all_to_all(outgoing, "ep", split_axis=0, concat_axis=0, tiled=True)
    sources, count, width_in = arrived.shape
    flat_rows = arrived.reshape(sources * count, width_in)
    gate_part = jnp.dot(flat_rows, w_gate[0], preferred_element_type=jnp.float32)
    up_part = jnp.dot(flat_rows, w_up[0], preferred_element_type=jnp.float32)
    hidden = (jax.nn.silu(gate_part) * up_part).astype(jnp.bfloat16)
    result = jnp.dot(hidden, w_down[0], preferred_element_type=jnp.float32).astype(jnp.bfloat16)
    returned = lax.all_to_all(
        result.reshape(sources, count, width_in), "ep", split_axis=0, concat_axis=0, tiled=True
    )
    picked = returned.reshape(experts_all * capacity, full_width)[dest_slot]
    weighted = picked.astype(jnp.float32) * gates.reshape(pair_count)[:, None]
    routed = jnp.sum(weighted.reshape(tok_rows, TOPK, full_width), axis=1).astype(jnp.bfloat16)
    shared = jnp.dot(
        shared_hidden,
        lax.all_gather(sh_down, "tp", axis=1, tiled=True),
        preferred_element_type=jnp.float32,
    ).astype(jnp.bfloat16)
    combined = routed.astype(jnp.float32) + shared.astype(jnp.float32)
    scale_out = lax.rsqrt(jnp.mean(combined * combined, axis=1, keepdims=True) + 1e-06)
    out_rows = (combined * scale_out * post_gain[None, :]).astype(jnp.bfloat16)
    return lax.all_to_all(out_rows, "tp", split_axis=1, concat_axis=0, tiled=True)


def solution(mesh):
    return jax.shard_map(
        per_device,
        mesh=mesh,
        in_specs=(
            P(("ep", "tp"), None),
            P(("ep", "tp"), None),
            P(("ep", "tp"), None),
            P(),
            P("ep", None, None),
            P("ep", None, None),
            P("ep", None, None),
            P("tp", None),
            P("tp", None),
            P(None, "tp"),
            P(),
        ),
        out_specs=P("ep", "tp"),
        check_vma=False,
    )
```

profile of v0, /device:TPU:1, one launch (start us, length us, event | category | flops | bytes accessed | tf_op | source)
XLA Modules:
  0.0 352.9 jit_solution(10643115844914263193)
XLA Ops:
  6.5 0.9 copy.21
  7.8 0.7 broadcast_multiply_fusion
  8.5 0.9 reduce-window.6
  9.4 0.2 slice_reduce_fusion
  9.8 0.1 mul.87
  10.1 2.9 scatter_custom_fusion
  13.0 1.4 fusion.7
  14.4 0.9 fusion.9
  15.4 0.9 copy-done.1
  16.3 3.3 gather_fusion
  19.6 4.2 %reshape.90 = bf16[48,10,2048]{2,1,0:T(8,128)(2,1)} reshape(bf16[480,2048]{1,0:T(8,128)(2,1)} %gather_fusion) | data formatting | bytes 3932160 | tf_op jit(solution)/shard_map/reshape | solution.py:40
  23.8 19.0 %all-to-all-start = ((bf16[48,10,2048]{2,1,0:T(8,128)(2,1)}), bf16[48,10,2048]{2,1,0:T(8,128)(2,1)}, u32[]{:S(2)}, u32[]{:S(2)}) async-start(bf16[48,10,2048]{2,1,0:T(8,128)(2,1)} %reshape.90), calls=%async_computation | async-start | bytes 6291456 | tf_op jit(solution)/shard_map/all_to_all | solution.py:41
  42.9 0.7 all-gather.4.cloned.1.call-update
  43.6 0.7 all-gather.6.cloned.1.call-update
  44.3 106.2 %all-to-all-done = bf16[48,10,2048]{2,1,0:T(8,128)(2,1)} async-done(((bf16[48,10,2048]{2,1,0:T(8,128)(2,1)}), bf16[48,10,2048]{2,1,0:T(8,128)(2,1)}, u32[]{:S(2)}, u32[]{:S(2)}) %all-to-all-start) | async-done | bytes 1966112 | tf_op jit(solution)/shard_map/all_to_all | solution.py:41
  150.5 4.2 %reshape.91 = bf16[480,2048]{1,0:T(8,128)(2,1)} reshape(bf16[48,10,2048]{2,1,0:T(8,128)(2,1)} %all-to-all-done) | data formatting | bytes 3932160 | tf_op jit(solution)/shard_map/reshape | solution.py:43
  154.7 4.3 %fusion.5 = f32[480,512]{1,0:T(8,128)} fusion(bf16[480,2048]{1,0:T(8,128)(2,1)} %reshape.91, bf16[1,2048,512]{2,1,0:T(8,128)(2,1)} %param.15), kind=kOutput, calls=%fused_computation.11 | convolution fusion | flops 1006632960 | bytes 5046272 | tf_op jit(solution)/shard_map/dot_general | solution.py:44
  159.1 6.0 %convolution_convert_fusion = bf16[480,2048]{1,0:T(8,128)(2,1)} fusion(bf16[1,512,2048]{2,1,0:T(8,128)(2,1)S(1)} %copy-done, bf16[480,2048]{1,0:T(8,128)(2,1)} %reshape.91, bf16[1,2048,512]{2,1,0:T(8,128)(2,1)} %param.16, f32[480,512]{1,0:T(8,128)} %fusion.5), kind=kOutput, calls=%fused_computation.4 | convolution fusion | flops 2015723520 | bytes 9109504 | tf_op jit(solution)/shard_map/dot_general | solution.py:47
  165.1 4.2 %reshape.92 = bf16[48,10,2048]{2,1,0:T(8,128)(2,1)} reshape(bf16[480,2048]{1,0:T(8,128)(2,1)} %convolution_convert_fusion) | data formatting | bytes 3932160 | tf_op jit(solution)/shard_map/reshape | solution.py:49
  169.3 6.8 %all-to-all-start.1 = ((bf16[48,10,2048]{2,1,0:T(8,128)(2,1)}), bf16[48,10,2048]{2,1,0:T(8,128)(2,1)}, u32[]{:S(2)}, u32[]{:S(2)}) async-start(bf16[48,10,2048]{2,1,0:T(8,128)(2,1)} %reshape.92), calls=%async_computation.1 | async-start | bytes 6291456 | tf_op jit(solution)/shard_map/all_to_all | solution.py:48
  176.1 0.2 all-gather.8.cloned.1.call-start
  176.4 0.5 all-gather.8.cloned.1.call-update
  177.1 2.2 fusion.39
  179.2 98.9 %all-to-all-done.1 = bf16[48,10,2048]{2,1,0:T(8,128)(2,1)} async-done(((bf16[48,10,2048]{2,1,0:T(8,128)(2,1)}), bf16[48,10,2048]{2,1,0:T(8,128)(2,1)}, u32[]{:S(2)}, u32[]{:S(2)}) %all-to-all-start.1) | async-done | bytes 1966112 | tf_op jit(solution)/shard_map/all_to_all | solution.py:48
  278.1 4.3 %reshape.93 = bf16[480,2048]{1,0:T(8,128)(2,1)} reshape(bf16[48,10,2048]{2,1,0:T(8,128)(2,1)} %all-to-all-done.1) | data formatting | bytes 3932160 | tf_op jit(solution)/shard_map/reshape | solution.py:51
  282.4 6.8 %gather_fusion.1 = bf16[384,2048]{1,0:T(8,128)(2,1)} fusion(bf16[480,2048]{1,0:T(8,128)(2,1)} %reshape.93, s32[1024]{0:T(1024)S(1)} %pad_clamp_fusion), kind=kCustom, calls=%fused_computation.1 | custom fusion | bytes 3147264 | tf_op jit(solution)/shard_map/gather | solution.py:51
  289.3 4.7 %reshape.94 = f32[192,2,2048]{2,1,0:T(2,128)} reshape(bf16[384,2048]{1,0:T(8,128)(2,1)} %gather_fusion.1) | data formatting | bytes 4718592 | tf_op jit(solution)/shard_map/convert_element_type | solution.py:52
  294.0 7.8 %multiply_reduce_fusion = bf16[192,2048]{1,0:T(8,128)(2,1)} fusion(f32[192,2,2048]{2,1,0:T(2,128)} %reshape.94, f32[192,2]{1,0:T(8,128)S(1)} %copy.24), kind=kLoop, calls=%fused_computation.3 | loop fusion | flops 1179648 | bytes 3933696 | tf_op jit(solution)/shard_map/reduce_sum | solution.py:53
  301.8 4.8 %multiply_reduce_fusion.1 = (f32[192]{0:T(256)S(1)}, f32[192,2048]{1,0:T(8,128)}) fusion(bf16[512,2048]{1,0:T(8,128)(2,1)} %all-gather.8.cloned.1.call-done, bf16[192,2048]{1,0:T(8,128)(2,1)S(1)} %copy-done.2, bf16[2048,512]{1,0:T(8,128)(2,1)} %all-gather.6.cloned.1.call-done, f32[192,512]{1,0:T(8,128)S(1)} %fusion.39, ...), kind=kOutput, calls=%fused_computation.19 | convolution fusion | flops 808255296 | bytes 7734016 | tf_op jit(solution)/shard_map/dot_general | solution.py:54
  306.5 1.7 copy_bitcast_fusion
  308.2 37.2 %all_to_all.29 = bf16[192,16,128]{2,0,1:T(8,128)(2,1)S(1)} all-to-all(bf16[192,16,128]{2,0,1:T(8,128)(2,1)S(1)} %copy_bitcast_fusion), channel_id=1, replica_groups=mesh['ep'=48,'tp'=16] {'tp'}, dimensions={1} | all-to-all | bytes 1572864 | tf_op jit(solution)/shard_map/all_to_all | solution.py:62
  345.5 0.9 copy.31
  (31 shorter events, 0.9 us)
Async XLA Ops:
  6.5 152.5 %copy-start = (bf16[1,512,2048]{2,1,0:T(8,128)(2,1)S(1)}, bf16[1,512,2048]{2,1,0:T(8,128)(2,1)}, u32[]{:S(2)}) copy-start(bf16[1,512,2048]{2,1,0:T(8,128)(2,1)} %param.17) | copy-start | bytes 6291460
  6.5 7.8 %copy-start.3 = (bf16[192,2048]{1,0:T(8,128)(2,1)S(1)}, bf16[192,2048]{1,0:T(8,128)(2,1)}, u32[]{:S(2)}) copy-start(bf16[192,2048]{1,0:T(8,128)(2,1)} %param.11) | copy-start | bytes 2359300
  15.3 0.9 copy-start.1
  23.8 126.7 %all-to-all-start = ((bf16[48,10,2048]{2,1,0:T(8,128)(2,1)}), bf16[48,10,2048]{2,1,0:T(8,128)(2,1)}, u32[]{:S(2)}, u32[]{:S(2)}) async-start(bf16[48,10,2048]{2,1,0:T(8,128)(2,1)} %reshape.90), calls=%async_computation | async-start | bytes 6291456 | tf_op jit(solution)/shard_map/all_to_all | solution.py:41
  42.8 134.2 %all-gather.4.cloned.1.call-start = ((), (), s32[]{:S(2)}) async-start(), calls=%async_computation.3 | async-start | bytes 2228224 | tf_op jit(solution)/shard_map/all_gather | solution.py:20
  43.6 258.2 %all-gather.6.cloned.1.call-start = ((), (), s32[]{:S(2)}) async-start(), calls=%async_computation.4 | async-start | bytes 2228224 | tf_op jit(solution)/shard_map/all_gather | solution.py:24
  169.3 7.6 %copy-start.5 = (f32[192,2]{0,1:T(2,128)S(1)}, f32[192,2]{0,1:T(2,128)}, u32[]{:S(2)}) copy-start(f32[192,2]{0,1:T(2,128)} %param.13) | copy-start | bytes 4612
  169.3 7.7 %copy-start.2 = (bf16[192,2048]{1,0:T(8,128)(2,1)S(1)}, bf16[192,2048]{1,0:T(8,128)(2,1)}, u32[]{:S(2)}) copy-start(bf16[192,2048]{1,0:T(8,128)(2,1)} %copy-done.1) | copy-start | bytes 2359300
  169.3 108.8 %all-to-all-start.1 = ((bf16[48,10,2048]{2,1,0:T(8,128)(2,1)}), bf16[48,10,2048]{2,1,0:T(8,128)(2,1)}, u32[]{:S(2)}, u32[]{:S(2)}) async-start(bf16[48,10,2048]{2,1,0:T(8,128)(2,1)} %reshape.92), calls=%async_computation.1 | async-start | bytes 6291456 | tf_op jit(solution)/shard_map/all_to_all | solution.py:48
  176.1 125.6 %all-gather.8.cloned.1.call-start = ((), (), s32[]{:S(2)}) async-start(), calls=%async_computation.5 | async-start | bytes 2228224 | tf_op jit(solution)/shard_map/all_gather | solution.py:56
  301.8 4.8 %copy-start.4 = (f32[2048]{0:T(1024)S(1)}, f32[2048]{0:T(1024)}, u32[]{:S(2)}) copy-start(f32[2048]{0:T(1024)} %param.21) | copy-start | bytes 24580
Sparse Core Ops, SparseCore 0:
  46.1 45.7 all-gather.3
  94.3 43.4 all-gather.5
  179.3 48.6 all-gather.7
where the time goes:
time: 354 us; the launch traced here: 353 us
  waiting for transfers between devices  207 us (58%)
  local copies, waits for them, and re-layouts  38.5 us (11%)
  blocking collectives  37.2 us (11%)
  starting transfers between devices  26.1 us (7%)
  matrix products  17.2 us (5%)
  other arithmetic  13.6 us (4%)
  between operations  13.3 us (4%)
    all_to_all x1, waiting for transfers between devices, per_device(): lax.all_to_all(outgoing, 'ep', split_axis=0, concat_axis=0, tiled=True)  106 us
    all_to_all x1, waiting for transfers between devices, per_device(): lax.all_to_all(result.reshape(sources, count, width_in), 'ep', split_axis...  98.9 us
    all_to_all x1, blocking collectives, per_device(): lax.all_to_all(out_rows, 'tp', split_axis=1, concat_axis=0, tiled=True)  37.2 us
    all_to_all x1, starting transfers between devices, per_device(): lax.all_to_all(outgoing, 'ep', split_axis=0, concat_axis=0, tiled=True)  19 us
    reduce_sum x1, other arithmetic, per_device(): jnp.sum(weighted.reshape(tok_rows, TOPK, full_width), axis=1)  7.76 us
  transfers between devices with their start and end apart: 5, of which 2 were waited for; matrix products, arithmetic and copies ran while one was open for 13% of the time, Pallas kernels for 0%

commit v1 on v0

--- a/solution.py
+++ b/solution.py
@@ -37,16 +37,17 @@
         jnp.full((experts_all * capacity,), tok_rows, jnp.int32).at[dest_slot].set(pair_token)
     )
     padded = jnp.concatenate([normed, jnp.zeros((1, full_width), jnp.bfloat16)], axis=0)
-    outgoing = padded[slot_token].reshape(experts_all, capacity, full_width)
+    lanes = 128
+    subrows = capacity * full_width // lanes
+    outgoing = padded[slot_token].reshape(experts_all, subrows, lanes)
     arrived = lax.all_to_all(outgoing, "ep", split_axis=0, concat_axis=0, tiled=True)
-    sources, count, width_in = arrived.shape
-    flat_rows = arrived.reshape(sources * count, width_in)
+    flat_rows = arrived.reshape(experts_all * capacity, full_width)
     gate_part = jnp.dot(flat_rows, w_gate[0], preferred_element_type=jnp.float32)
     up_part = jnp.dot(flat_rows, w_up[0], preferred_element_type=jnp.float32)
     hidden = (jax.nn.silu(gate_part) * up_part).astype(jnp.bfloat16)
     result = jnp.dot(hidden, w_down[0], preferred_element_type=jnp.float32).astype(jnp.bfloat16)
     returned = lax.all_to_all(
-        result.reshape(sources, count, width_in), "ep", split_axis=0, concat_axis=0, tiled=True
+        result.reshape(experts_all, subrows, lanes), "ep", split_axis=0, concat_axis=0, tiled=True
     )
     picked = returned.reshape(experts_all * capacity, full_width)[dest_slot]
     weighted = picked.astype(jnp.float32) * gates.reshape(pair_count)[:, None]

time: 354 us -> 278 us (0.79)
  waiting for transfers between devices: 207 us -> 132 us
    all_to_all x1, waiting for transfers between devices: 106 us -> 66.3 us  [per_device(): lax.all_to_all(outgoing, 'ep', split_axis=0, concat_axis=0, tiled=True)]
    all_to_all x1, waiting for transfers between devices: 98.9 us -> 63.7 us  [per_device(): lax.all_to_all(result.reshape(experts_all, subrows, lanes), 'ep', split_a...]
  transfers between devices with their start and end apart: 5 -> 5, of which waited for: 2 -> 2; matrix products, arithmetic and copies ran while one was open for 13% -> 16% of each run, Pallas kernels for 0% -> 0%
where the time goes in v1:
time: 278 us; the launch traced here: 277 us
  waiting for transfers between devices  132 us (47%)
  local copies, waits for them, and re-layouts  37.7 us (14%)
  blocking collectives  35 us (13%)
  starting transfers between devices  28 us (10%)
  matrix products  17.3 us (6%)
  other arithmetic  13.6 us (5%)
  between operations  13.3 us (5%)
    all_to_all x1, waiting for transfers between devices, per_device(): lax.all_to_all(outgoing, 'ep', split_axis=0, concat_axis=0, tiled=True)  66.3 us
    all_to_all x1, waiting for transfers between devices, per_device(): lax.all_to_all(result.reshape(experts_all, subrows, lanes), 'ep', split_a...  63.7 us
    all_to_all x1, blocking collectives, per_device(): lax.all_to_all(out_rows, 'tp', split_axis=1, concat_axis=0, tiled=True)  35 us
    all_to_all x1, starting transfers between devices, per_device(): lax.all_to_all(outgoing, 'ep', split_axis=0, concat_axis=0, tiled=True)  19 us
    all_to_all x1, starting transfers between devices, per_device(): lax.all_to_all(result.reshape(experts_all, subrows, lanes), 'ep', split_a...  8.75 us
    reduce_sum x1, other arithmetic, per_device(): jnp.sum(weighted.reshape(tok_rows, TOPK, full_width), axis=1)  7.76 us
    gather x1, local copies, waits for them, and re-layouts, per_device(): picked = returned.reshape(experts_all * capacity, full_width)[dest_slot]  6.84 us
    dot_general x1, matrix products, per_device(): jnp.dot(hidden, w_down[0], preferred_element_type=jnp.float32)  6.11 us
  transfers between devices with their start and end apart: 5, of which 2 were waited for; matrix products, arithmetic and copies ran while one was open for 16% of the time, Pallas kernels for 0%

profile of v1, /device:TPU:1, one launch (start us, length us, event | category | flops | bytes accessed | tf_op | source)
XLA Modules:
  0.0 276.9 jit_solution(10376689502337234208)
XLA Ops:
  6.5 0.9 copy.21
  7.8 0.7 broadcast_multiply_fusion
  8.5 0.9 reduce-window.6
  9.4 0.2 slice_reduce_fusion
  9.8 0.1 mul.87
  10.1 2.9 %scatter_custom_fusion = s32[480]{0:T(512)S(1)} fusion(s32[384]{0:T(512)S(1)} %fusion.34, s32[384]{0:T(512)S(1)} %add_select_fusion, s32[]{:T(128)} %constant.38.clone.1), kind=kCustom, calls=%fused_computation.56 | custom fusion | bytes 1924 | tf_op jit(solution)/shard_map/scatter | solution.py:37
  13.0 1.4 fusion.7
  14.4 0.9 fusion.9
  15.4 0.9 copy-done.1
  16.3 3.3 %gather_fusion = bf16[480,2048]{1,0:T(8,128)(2,1)} fusion(bf16[193,2048]{1,0:T(8,128)(2,1)S(1)} %concatenate.3, s32[1024]{0:T(1024)S(1)} %pad_clamp_fusion.1), kind=kCustom, calls=%fused_computation | custom fusion | bytes 3934080 | tf_op jit(solution)/shard_map/gather | solution.py:42
  19.6 4.1 %reshape.90 = bf16[48,160,128]{2,1,0:T(8,128)(2,1)} reshape(bf16[480,2048]{1,0:T(8,128)(2,1)} %gather_fusion) | data formatting | bytes 3932160 | tf_op jit(solution)/shard_map/reshape | solution.py:42
  23.6 19.0 %all-to-all-start = ((bf16[48,160,128]{2,1,0:T(8,128)(2,1)}), bf16[48,160,128]{2,1,0:T(8,128)(2,1)}, u32[]{:S(2)}, u32[]{:S(2)}) async-start(bf16[48,160,128]{2,1,0:T(8,128)(2,1)} %reshape.90), calls=%async_computation | async-start | bytes 3932160 | tf_op jit(solution)/shard_map/all_to_all | solution.py:43
  42.7 0.7 all-gather.4.cloned.1.call-update
  43.4 0.7 all-gather.6.cloned.1.call-update
  44.1 66.3 %all-to-all-done = bf16[48,160,128]{2,1,0:T(8,128)(2,1)} async-done(((bf16[48,160,128]{2,1,0:T(8,128)(2,1)}), bf16[48,160,128]{2,1,0:T(8,128)(2,1)}, u32[]{:S(2)}, u32[]{:S(2)}) %all-to-all-start) | async-done | bytes 1966112 | tf_op jit(solution)/shard_map/all_to_all | solution.py:43
  110.5 4.0 %reshape.91 = bf16[480,2048]{1,0:T(8,128)(2,1)} reshape(bf16[48,160,128]{2,1,0:T(8,128)(2,1)} %all-to-all-done) | data formatting | bytes 3932160 | tf_op jit(solution)/shard_map/reshape | solution.py:44
  114.5 4.4 %fusion.5 = f32[480,512]{1,0:T(8,128)} fusion(bf16[480,2048]{1,0:T(8,128)(2,1)} %reshape.91, bf16[1,2048,512]{2,1,0:T(8,128)(2,1)} %param.15), kind=kOutput, calls=%fused_computation.11 | convolution fusion | flops 1006632960 | bytes 5046272 | tf_op jit(solution)/shard_map/dot_general | solution.py:45
  118.9 6.1 %convolution_convert_fusion = bf16[480,2048]{1,0:T(8,128)(2,1)} fusion(bf16[1,512,2048]{2,1,0:T(8,128)(2,1)S(1)} %copy-done, bf16[480,2048]{1,0:T(8,128)(2,1)} %reshape.91, bf16[1,2048,512]{2,1,0:T(8,128)(2,1)} %param.16, f32[480,512]{1,0:T(8,128)} %fusion.5), kind=kOutput, calls=%fused_computation.4 | convolution fusion | flops 2015723520 | bytes 9109504 | tf_op jit(solution)/shard_map/dot_general | solution.py:48
  125.0 4.1 %reshape.92 = bf16[48,160,128]{2,1,0:T(8,128)(2,1)} reshape(bf16[480,2048]{1,0:T(8,128)(2,1)} %convolution_convert_fusion) | data formatting | bytes 3932160 | tf_op jit(solution)/shard_map/reshape | solution.py:50
  129.2 8.7 %all-to-all-start.1 = ((bf16[48,160,128]{2,1,0:T(8,128)(2,1)}), bf16[48,160,128]{2,1,0:T(8,128)(2,1)}, u32[]{:S(2)}, u32[]{:S(2)}) async-start(bf16[48,160,128]{2,1,0:T(8,128)(2,1)} %reshape.92), calls=%async_computation.1 | async-start | bytes 3932160 | tf_op jit(solution)/shard_map/all_to_all | solution.py:49
  137.9 0.2 all-gather.8.cloned.1.call-start
  138.1 0.5 all-gather.8.cloned.1.call-update
  138.8 2.2 fusion.39
  141.0 63.7 %all-to-all-done.1 = bf16[48,160,128]{2,1,0:T(8,128)(2,1)} async-done(((bf16[48,160,128]{2,1,0:T(8,128)(2,1)}), bf16[48,160,128]{2,1,0:T(8,128)(2,1)}, u32[]{:S(2)}, u32[]{:S(2)}) %all-to-all-start.1) | async-done | bytes 1966112 | tf_op jit(solution)/shard_map/all_to_all | solution.py:49
  204.7 4.0 %reshape.93 = bf16[480,2048]{1,0:T(8,128)(2,1)} reshape(bf16[48,160,128]{2,1,0:T(8,128)(2,1)} %all-to-all-done.1) | data formatting | bytes 3932160 | tf_op jit(solution)/shard_map/reshape | solution.py:52
  208.8 6.8 %gather_fusion.1 = bf16[384,2048]{1,0:T(8,128)(2,1)} fusion(bf16[480,2048]{1,0:T(8,128)(2,1)} %reshape.93, s32[1024]{0:T(1024)S(1)} %pad_clamp_fusion), kind=kCustom, calls=%fused_computation.1 | custom fusion | bytes 3147264 | tf_op jit(solution)/shard_map/gather | solution.py:52
  215.6 4.8 %reshape.94 = f32[192,2,2048]{2,1,0:T(2,128)} reshape(bf16[384,2048]{1,0:T(8,128)(2,1)} %gather_fusion.1) | data formatting | bytes 4718592 | tf_op jit(solution)/shard_map/convert_element_type | solution.py:53
  220.3 7.8 %multiply_reduce_fusion = bf16[192,2048]{1,0:T(8,128)(2,1)} fusion(f32[192,2,2048]{2,1,0:T(2,128)} %reshape.94, f32[192,2]{1,0:T(8,128)S(1)} %copy.24), kind=kLoop, calls=%fused_computation.3 | loop fusion | flops 1179648 | bytes 3933696 | tf_op jit(solution)/shard_map/reduce_sum | solution.py:54
  228.1 4.7 %multiply_reduce_fusion.1 = (f32[192]{0:T(256)S(1)}, f32[192,2048]{1,0:T(8,128)}) fusion(bf16[512,2048]{1,0:T(8,128)(2,1)} %all-gather.8.cloned.1.call-done, bf16[192,2048]{1,0:T(8,128)(2,1)S(1)} %copy-done.2, bf16[2048,512]{1,0:T(8,128)(2,1)} %all-gather.6.cloned.1.call-done, f32[192,512]{1,0:T(8,128)S(1)} %fusion.39, ...), kind=kOutput, calls=%fused_computation.19 | convolution fusion | flops 808255296 | bytes 7734016 | tf_op jit(solution)/shard_map/dot_general | solution.py:55
  232.8 1.7 copy_bitcast_fusion
  234.5 35.0 %all_to_all.29 = bf16[192,16,128]{2,0,1:T(8,128)(2,1)S(1)} all-to-all(bf16[192,16,128]{2,0,1:T(8,128)(2,1)S(1)} %copy_bitcast_fusion), channel_id=1, replica_groups=mesh['ep'=48,'tp'=16] {'tp'}, dimensions={1} | all-to-all | bytes 1572864 | tf_op jit(solution)/shard_map/all_to_all | solution.py:63
  269.4 0.9 copy.31
  (31 shorter events, 0.9 us)
Async XLA Ops:
  6.5 112.4 %copy-start = (bf16[1,512,2048]{2,1,0:T(8,128)(2,1)S(1)}, bf16[1,512,2048]{2,1,0:T(8,128)(2,1)}, u32[]{:S(2)}) copy-start(bf16[1,512,2048]{2,1,0:T(8,128)(2,1)} %param.17) | copy-start | bytes 6291460
  6.5 7.8 %copy-start.3 = (bf16[192,2048]{1,0:T(8,128)(2,1)S(1)}, bf16[192,2048]{1,0:T(8,128)(2,1)}, u32[]{:S(2)}) copy-start(bf16[192,2048]{1,0:T(8,128)(2,1)} %param.11) | copy-start | bytes 2359300
  15.3 0.9 copy-start.1
  23.6 86.8 %all-to-all-start = ((bf16[48,160,128]{2,1,0:T(8,128)(2,1)}), bf16[48,160,128]{2,1,0:T(8,128)(2,1)}, u32[]{:S(2)}, u32[]{:S(2)}) async-start(bf16[48,160,128]{2,1,0:T(8,128)(2,1)} %reshape.90), calls=%async_computation | async-start | bytes 3932160 | tf_op jit(solution)/shard_map/all_to_all | solution.py:43
  42.7 96.2 %all-gather.4.cloned.1.call-start = ((), (), s32[]{:S(2)}) async-start(), calls=%async_computation.3 | async-start | bytes 2228224 | tf_op jit(solution)/shard_map/all_gather | solution.py:20
  43.4 184.7 %all-gather.6.cloned.1.call-start = ((), (), s32[]{:S(2)}) async-start(), calls=%async_computation.4 | async-start | bytes 2228224 | tf_op jit(solution)/shard_map/all_gather | solution.py:24
  129.2 9.5 %copy-start.5 = (f32[192,2]{0,1:T(2,128)S(1)}, f32[192,2]{0,1:T(2,128)}, u32[]{:S(2)}) copy-start(f32[192,2]{0,1:T(2,128)} %param.13) | copy-start | bytes 4612
  129.2 9.7 %copy-start.2 = (bf16[192,2048]{1,0:T(8,128)(2,1)S(1)}, bf16[192,2048]{1,0:T(8,128)(2,1)}, u32[]{:S(2)}) copy-start(bf16[192,2048]{1,0:T(8,128)(2,1)} %copy-done.1) | copy-start | bytes 2359300
  129.2 75.6 %all-to-all-start.1 = ((bf16[48,160,128]{2,1,0:T(8,128)(2,1)}), bf16[48,160,128]{2,1,0:T(8,128)(2,1)}, u32[]{:S(2)}, u32[]{:S(2)}) async-start(bf16[48,160,128]{2,1,0:T(8,128)(2,1)} %reshape.92), calls=%async_computation.1 | async-start | bytes 3932160 | tf_op jit(solution)/shard_map/all_to_all | solution.py:49
  137.9 90.2 %all-gather.8.cloned.1.call-start = ((), (), s32[]{:S(2)}) async-start(), calls=%async_computation.5 | async-start | bytes 2228224 | tf_op jit(solution)/shard_map/all_gather | solution.py:57
  228.1 4.7 %copy-start.4 = (f32[2048]{0:T(1024)S(1)}, f32[2048]{0:T(1024)}, u32[]{:S(2)}) copy-start(f32[2048]{0:T(1024)} %param.21) | copy-start | bytes 24580
Sparse Core Ops, SparseCore 0:
  45.9 45.8 all-gather.3
  94.1 43.5 all-gather.5
  141.1 48.6 all-gather.7

commit v2 on v0

v2 whole, which is shorter than its diff:
```python
import functools

import jax
import jax.numpy as jnp
from jax import lax
from jax.experimental import pallas as pl
from jax.experimental.pallas import tpu as pltpu
from jax.sharding import PartitionSpec as P

TOPK = 2
LANES = 128
TILE = 16
MESH = pl.DeviceIdType.MESH
F32 = jnp.float32
BF16 = jnp.bfloat16


def dot(a, b):
    return jnp.dot(a, b, preferred_element_type=F32)


def silu_mul(gate, up):
    return (gate / (1.0 + jnp.exp(-gate)) * up).astype(BF16)


def offset_at(place, n_ep):
    near = n_ep - 1 - place
    odd = lax.rem(near, 2)
    return odd * ((near + 1) // 2) + (1 - odd) * (n_ep - near // 2)


def rows_to_tiles(swap, read, width):
    stacked = jnp.concatenate(
        [read(pl.ds(LANES * j, LANES)) for j in range(width // LANES)], axis=0
    )
    return dot(swap, stacked).astype(BF16).reshape(TILE, TILE, LANES)


def tiles_to_rows(swap, tiles, write):
    flat = dot(swap, tiles.reshape(TILE * TILE, LANES)).astype(BF16)
    for j in range(TILE):
        write(pl.ds(LANES * j, LANES), flat[TILE * j : TILE * (j + 1), :])


def kernel(
    n_ep, n_tp, cap, chunk,
    tokens, routes, gates, pre_gain, w_gate, w_up, w_down, sh_gate, sh_up, sh_down, post_gain,
    out,
    normed, pick, swap, flat, outgoing, arrived, results, returned,
    wg, wu, wd, xs, rs, all_gate, all_up, all_down, shared, combined, out_blocks, out_landed,
    w_sem, send_sem, arrive_sem, back_send, back_recv,
    sh_send, sh_recv, pair_send, pair_recv, out_send, out_recv, last_sem,
):
    me, tp = lax.axis_index("ep"), lax.axis_index("tp")
    core, row = lax.rem(tp, 2), tp // 2
    n_row = n_tp // 2
    rows, width = tokens.shape
    slots = n_ep * cap
    n_chunks = n_ep // chunk
    span = chunk * cap
    out_width = width // n_tp

    barrier = pltpu.get_barrier_semaphore()

    def greet_ep(i, carry):
        pl.semaphore_signal(
            barrier, inc=1, device_id=(lax.rem(me + i, n_ep), tp), device_id_type=MESH
        )
        return carry

    def greet_tp(i, carry):
        pl.semaphore_signal(
            barrier, inc=1, device_id=(me, lax.rem(tp + i, n_tp)), device_id_type=MESH
        )
        return carry

    lax.fori_loop(1, n_ep, greet_ep, 0)
    lax.fori_loop(1, n_tp, greet_tp, 0)

    weight_copies = [
        pltpu.make_async_copy(source, target, w_sem.at[i])
        for i, (source, target) in enumerate(((w_gate, wg), (w_up, wu), (w_down, wd)))
    ]
    for copy in weight_copies:
        copy.start()

    def norm_rows(i, carry):
        at = pl.ds(pl.multiple_of(i * TILE, TILE), TILE)
        values = tokens[at, :].astype(F32)
        scale = lax.rsqrt(jnp.mean(values * values, axis=1, keepdims=True) + 1e-06)
        normed[at, :] = (values * scale * pre_gain[...]).astype(BF16)
        return carry

    lax.fori_loop(0, rows // TILE, norm_rows, 0)

    expert = lax.broadcasted_iota(jnp.int32, (rows, LANES), 1)
    first, second = routes[:, 0:1], routes[:, 1:2]
    match0 = jnp.where(first == expert, 1.0, 0.0).astype(F32)
    match1 = jnp.where(second == expert, 1.0, 0.0).astype(F32)
    earlier = jnp.where(
        lax.broadcasted_iota(jnp.int32, (rows, rows), 1)
        < lax.broadcasted_iota(jnp.int32, (rows, rows), 0),
        1.0,
        0.0,
    ).astype(BF16)
    before = dot(earlier, (match0 + match1).astype(BF16))
    place0 = first.astype(F32) * cap + jnp.sum(before * match0, axis=1, keepdims=True)
    place1 = second.astype(F32) * cap + jnp.sum(before * match1, axis=1, keepdims=True)
    slot = lax.broadcasted_iota(jnp.int32, (rows, slots), 1).astype(F32)
    pick0 = jnp.where(slot == place0, 1.0, 0.0)
    pick1 = jnp.where(slot == place1, 1.0, 0.0)
    pick[0:rows, :] = pick0.astype(BF16)
    pick[rows : 2 * rows, :] = pick1.astype(BF16)
    either = (pick0 + pick1).astype(BF16)

    side = TILE * TILE
    to = lax.broadcasted_iota(jnp.int32, (side, side), 0)
    come = lax.broadcasted_iota(jnp.int32, (side, side), 1)
    swap[...] = jnp.where(come == lax.rem(to, TILE) * TILE + to // TILE, 1.0, 0.0).astype(BF16)

    wide = 2 * LANES
    for j in range(width // wide):
        columns = pl.ds(j * wide, wide)
        flat[:, columns] = lax.dot_general(
            either, normed[:, columns], (((0,), (0,)), ((), ())), preferred_element_type=F32
        ).astype(BF16)

    def pack(i, carry):
        at = pl.ds(pl.multiple_of(i * TILE, TILE), TILE)
        outgoing[at] = rows_to_tiles(swap[...], lambda columns: flat[at, columns], width)
        return carry

    lax.fori_loop(0, slots // TILE, pack, 0)

    pl.semaphore_wait(barrier, n_ep - 1 + n_tp - 1)

    def send(place, carry):
        target = lax.rem(me + offset_at(place, n_ep), n_ep)
        pltpu.make_async_remote_copy(
            src_ref=outgoing.at[pl.ds(target * cap, cap)],
            dst_ref=arrived.at[pl.ds(place * cap, cap)],
            send_sem=send_sem,
            recv_sem=arrive_sem.at[place // chunk],
            device_id=(target, tp),
            device_id_type=MESH,
        ).start()
        return carry

    lax.fori_loop(0, n_ep - 1, send, 0)
    arrived[pl.ds((n_ep - 1) * cap, cap)] = outgoing[pl.ds(me * cap, cap)]

    shared_parts = ((sh_gate, all_gate), (sh_up, all_up), (sh_down, all_down))
    for n, (block, whole) in enumerate(shared_parts):

        def share(i, carry, n=n, block=block, whole=whole):
            pltpu.make_async_remote_copy(
                src_ref=block,
                dst_ref=whole.at[core, row],
                send_sem=sh_send.at[n],
                recv_sem=sh_recv.at[n],
                device_id=(me, lax.rem(tp + 2 * i, n_tp)),
                device_id_type=MESH,
            ).start()
            return carry

        lax.fori_loop(1, n_row, share, 0)
        whole[core, row] = block[...]

    for copy in weight_copies:
        copy.wait()

    def arrival(n, at):
        return pltpu.make_async_remote_copy(
            src_ref=arrived.at[at], dst_ref=arrived.at[at], send_sem=send_sem,
            recv_sem=arrive_sem.at[n], device_id=(me, tp), device_id_type=MESH,
        )

    def expert_step(n, carry):
        base = pl.multiple_of(n * span, TILE)

        @pl.when(n < n_chunks - 1)
        def _():
            arrival(n, pl.ds(base, span)).wait_recv()

        @pl.when(n == n_chunks - 1)
        def _():
            arrival(n, pl.ds(base, span - cap)).wait_recv()

        for g in range(span // TILE):
            at = pl.ds(g * TILE, TILE)

            def put(columns, values, at=at):
                xs[at, columns] = values

            tiles_to_rows(swap[...], arrived[pl.ds(base + g * TILE, TILE)], put)
        taken = xs[...]
        hidden = silu_mul(dot(taken, wg[...]), dot(taken, wu[...]))
        for j in range(width // 512):
            columns = pl.ds(j * 512, 512)
            rs[:, columns] = dot(hidden, wd[:, columns]).astype(BF16)
        for g in range(span // TILE):
            at = pl.ds(g * TILE, TILE)
            results[pl.ds(base + g * TILE, TILE)] = rows_to_tiles(
                swap[...], lambda columns, at=at: rs[at, columns], width
            )

        def send_back(i, inner):
            place = n * chunk + i
            target = lax.rem(me + n_ep - offset_at(place, n_ep), n_ep)

            @pl.when(place < n_ep - 1)
            def _():
                pltpu.make_async_remote_copy(
                    src_ref=results.at[pl.ds(place * cap, cap)],
                    dst_ref=returned.at[pl.ds(me * cap, cap)],
                    send_sem=back_send,
                    recv_sem=back_recv,
                    device_id=(target, tp),
                    device_id_type=MESH,
                ).start()

            return inner

        lax.fori_loop(0, chunk, send_back, 0)
        return carry

    lax.fori_loop(0, n_chunks, expert_step, 0)
    returned[pl.ds(me * cap, cap)] = results[pl.ds((n_ep - 1) * cap, cap)]

    pair = tp + 1 - 2 * core
    pairs = []
    for n, (block, whole) in enumerate(shared_parts):
        most = whole.at[core, pl.ds(0, n_row - 1)]
        pltpu.make_async_remote_copy(
            src_ref=most, dst_ref=most, send_sem=sh_send.at[n], recv_sem=sh_recv.at[n],
            device_id=(me, tp), device_id_type=MESH,
        ).wait()
        copy = pltpu.make_async_remote_copy(
            src_ref=whole.at[core], dst_ref=whole.at[core], send_sem=pair_send.at[n],
            recv_sem=pair_recv.at[n], device_id=(me, pair), device_id_type=MESH,
        )
        copy.start()
        pairs.append(copy)
    for copy in pairs:
        copy.wait()

    ff = sh_gate.shape[1]
    depth = sh_gate.shape[0]
    gate_sum = jnp.zeros((rows, ff), F32)
    up_sum = jnp.zeros((rows, ff), F32)
    for r in range(n_row):
        part = normed[:, pl.ds(2 * r * depth, 2 * depth)]
        gate_sum += dot(part, jnp.concatenate([all_gate[0, r], all_gate[1, r]], axis=0))
        up_sum += dot(part, jnp.concatenate([all_up[0, r], all_up[1, r]], axis=0))
    shared_hidden = silu_mul(gate_sum, up_sum)
    for r in range(n_row):
        both = jnp.concatenate([all_down[0, r], all_down[1, r]], axis=1)
        shared[:, pl.ds(2 * r * out_width, 2 * out_width)] = dot(shared_hidden, both).astype(BF16)

    rest = pl.ds(0, (n_ep - 1) * cap)
    pltpu.make_async_remote_copy(
        src_ref=results.at[rest], dst_ref=returned.at[rest], send_sem=back_send,
        recv_sem=back_recv, device_id=(me, tp), device_id_type=MESH,
    ).wait()

    def unpack(i, carry):
        at = pl.ds(pl.multiple_of(i * TILE, TILE), TILE)

        def put(columns, values):
            flat[at, columns] = values

        tiles_to_rows(swap[...], returned[at], put)
        return carry

    lax.fori_loop(0, slots // TILE, unpack, 0)
    weight0, weight1 = gates[:, 0:1], gates[:, 1:2]
    squares = jnp.zeros((rows, LANES), F32)
    for j in range(width // wide):
        columns = pl.ds(j * wide, wide)
        picked = dot(pick[...], flat[:, columns])
        routed = (weight0 * picked[0:rows] + weight1 * picked[rows : 2 * rows]).astype(BF16)
        total = routed.astype(F32) + shared[:, columns].astype(F32)
        combined[:, columns] = total
        squares += total[:, 0:LANES] * total[:, 0:LANES] + total[:, LANES:] * total[:, LANES:]
    scale_out = lax.rsqrt(jnp.sum(squares, axis=1, keepdims=True) * (1.0 / width) + 1e-06)
    for j in range(n_tp):
        columns = pl.ds(j * out_width, out_width)
        out_blocks[j] = (combined[:, columns] * scale_out * post_gain[:, columns]).astype(BF16)

    def send_out(i, carry):
        target = lax.rem(tp + i, n_tp)
        pltpu.make_async_remote_copy(
            src_ref=out_blocks.at[target],
            dst_ref=out_landed.at[tp],
            send_sem=out_send,
            recv_sem=out_recv,
            device_id=(me, target),
            device_id_type=MESH,
        ).start()
        return carry

    lax.fori_loop(1, n_tp, send_out, 0)
    out_landed[tp] = out_blocks[tp]

    pltpu.make_async_remote_copy(
        src_ref=outgoing.at[rest], dst_ref=arrived.at[rest], send_sem=send_sem,
        recv_sem=back_recv, device_id=(me, tp), device_id_type=MESH,
    ).wait_send()
    others = pl.ds(0, n_tp - 1)
    pltpu.make_async_remote_copy(
        src_ref=out_blocks.at[others], dst_ref=out_landed.at[others], send_sem=out_send,
        recv_sem=out_recv, device_id=(me, tp), device_id_type=MESH,
    ).wait()
    last = pltpu.make_async_copy(out_landed, out, last_sem)
    last.start()
    last.wait()


def per_device(
    tokens, routes, gates, pre_gain, w_gate, w_up, w_down, sh_gate, sh_up, sh_down, post_gain
):
    rows, width = tokens.shape
    n_ep, n_tp = lax.axis_size("ep"), lax.axis_size("tp")
    ff = w_gate.shape[2]
    cap = max(2, 4 * rows * TOPK // (3 * n_ep))
    chunk = next(c for c in range(2, n_ep) if n_ep % c == 0 and c * cap % TILE == 0)
    slots = n_ep * cap
    n_row = n_tp // 2
    depth, sh_ff = sh_gate.shape
    out_width = width // n_tp
    tiles = pltpu.VMEM((slots, TILE, LANES), BF16)
    vmem = pl.BlockSpec(memory_space=pltpu.VMEM)
    anywhere = pl.BlockSpec(memory_space=pl.ANY)
    dma = pltpu.SemaphoreType.DMA
    result = pl.pallas_call(
        functools.partial(kernel, n_ep, n_tp, cap, chunk),
        out_shape=jax.ShapeDtypeStruct((n_tp, rows, out_width), BF16),
        in_specs=[vmem] * 4 + [anywhere] * 3 + [vmem] * 4,
        out_specs=anywhere,
        scratch_shapes=[
            pltpu.VMEM((rows, width), BF16),
            pltpu.VMEM((2 * rows, slots), BF16),
            pltpu.VMEM((TILE * TILE, TILE * TILE), BF16),
            pltpu.VMEM((slots, width), BF16),
            tiles, tiles, tiles, tiles,
            pltpu.VMEM((width, ff), BF16),
            pltpu.VMEM((width, ff), BF16),
            pltpu.VMEM((ff, width), BF16),
            pltpu.VMEM((chunk * cap, width), BF16),
            pltpu.VMEM((chunk * cap, width), BF16),
            pltpu.VMEM((2, n_row, depth, sh_ff), BF16),
            pltpu.VMEM((2, n_row, depth, sh_ff), BF16),
            pltpu.VMEM((2, n_row, sh_ff, out_width), BF16),
            pltpu.VMEM((rows, width), BF16),
            pltpu.VMEM((rows, width), F32),
            pltpu.VMEM((n_tp, rows, out_width), BF16),
            pltpu.VMEM((n_tp, rows, out_width), BF16),
            dma((3,)), dma, dma((n_ep // chunk,)), dma, dma,
            dma((3,)), dma((3,)), dma((3,)), dma((3,)), dma, dma, dma,
        ],
        compiler_params=pltpu.CompilerParams(
            collective_id=0, has_side_effects=True, vmem_limit_bytes=60 * 1024 * 1024
        ),
    )(
        tokens, routes, gates, pre_gain.reshape(1, width),
        w_gate.reshape(width, ff), w_up.reshape(width, ff), w_down.reshape(ff, width),
        sh_gate, sh_up, sh_down, post_gain.reshape(1, width),
    )
    return result.reshape(n_tp * rows, out_width)


def solution(mesh):
    return jax.shard_map(
        per_device,
        mesh=mesh,
        in_specs=(
            P(("ep", "tp"), None),
            P(("ep", "tp"), None),
            P(("ep", "tp"), None),
            P(),
            P("ep", None, None),
            P("ep", None, None),
            P("ep", None, None),
            P("tp", None),
            P("tp", None),
            P(None, "tp"),
            P(),
        ),
        out_specs=P("ep", "tp"),
        check_vma=False,
    )
```

time: 354 us -> 191 us (0.54)
  waiting for transfers between devices: 207 us -> 0 us
  Pallas kernels: 0 us -> 185 us
  blocking collectives: 37.2 us -> 0 us
  local copies, waits for them, and re-layouts: 38.5 us -> 4.94 us
  starting transfers between devices: 26.1 us -> 0 us
  matrix products: 17.2 us -> 0 us
  other arithmetic: 13.6 us -> 0 us
  between operations: 13.3 us -> 0.01 us
    all_to_all x2 -> x0, waiting for transfers between devices: 205 us -> none  [the longest x1 106 us: per_device(): lax.all_to_all(outgoing, 'ep', split_axis=0, concat_axis=0, tiled=True)]
    pallas_call x0 -> x1, Pallas kernels: none -> 185 us  [per_device(): pl.pallas_call(functools.partial(kernel, n_ep, n_tp, cap, chunk), out_sha...]
    all_to_all x1 -> x0, blocking collectives: 37.2 us -> none  [per_device(): lax.all_to_all(out_rows, 'tp', split_axis=1, concat_axis=0, tiled=True)]
    all_to_all x2 -> x0, starting transfers between devices: 25.8 us -> none  [the longest x1 19 us: per_device(): lax.all_to_all(outgoing, 'ep', split_axis=0, concat_axis=0, tiled=True)]
    dot_general x4 -> x0, matrix products: 17.2 us -> none  [the longest x1 6 us: per_device(): jnp.dot(hidden, w_down[0], preferred_element_type=jnp.float32)]
    reshape x4 -> x0, local copies, waits for them, and re-layouts: 17 us -> none  [the longest x1 4.3 us: per_device(): picked = returned.reshape(experts_all * capacity, full_width)[dest_slot]]
    gather x2 -> x0, local copies, waits for them, and re-layouts: 10.1 us -> none  [the longest x1 6.85 us: per_device(): picked = returned.reshape(experts_all * capacity, full_width)[dest_slot]]
    reduce_sum x3 -> x0, other arithmetic: 9.23 us -> none  [the longest x1 7.76 us: per_device(): jnp.sum(weighted.reshape(tok_rows, TOPK, full_width), axis=1)]
  transfers between devices with their start and end apart: 5 -> 0, of which waited for: 2 -> 0; matrix products, arithmetic and copies ran while one was open for 13% -> 0% of each run, Pallas kernels for 0% -> 0%
where the time goes in v2:
time: 191 us; the launch traced here: 190 us
  Pallas kernels  185 us (97%)
  local copies, waits for them, and re-layouts  4.94 us (3%)
    pallas_call x1, Pallas kernels, per_device(): pl.pallas_call(functools.partial(kernel, n_ep, n_tp, cap, chunk), out_sha...  185 us
    unnamed x3, local copies, waits for them, and re-layouts  4.94 us

profile of v2, /device:TPU:1, one launch (start us, length us, event | category | flops | bytes accessed | tf_op | source)
XLA Modules:
  0.0 190.4 jit_solution(6116462515845545112)
XLA Ops:
  0.0 1.4 copy.12.routes
  1.4 1.4 copy.13.gates
  2.9 185.4 %shard_map.109 = bf16[16,192,128]{2,1,0:T(8,128)(2,1)} custom-call(bf16[192,2048]{1,0:T(8,128)(2,1)} %tokens.1, s32[192,2]{1,0:T(8,128)} %copy.12.routes, f32[192,2]{1,0:T(8,128)} %copy.13.gates, f32[1,2048]{1,0:T(1,128)} %bitcast.10, bf16[2048,512]{1,0:T(8,128)(2,1)} %bitcast.7, bf16[2048,512]{1,0:T(8,128)(2,1)} %bitcast.8, bf16[512,2048]{1,0:T(8,128)(2,1)} %bitcast.9, ...), custom_call_target="tpu_custom_call" | custom-call | tf_op jit(solution)/shard_map/pallas_call | solution.py:335
  188.3 2.1 %copy.15 = bf16[3072,128]{1,0:T(8,128)(2,1)} copy(bf16[3072,128]{1,0:T(8,128)(2,1)} %bitcast.6) | data formatting | bytes 1572864

commit v3 on v0

v3 whole, which is shorter than its diff:
```python
import functools

import jax
import jax.numpy as jnp
from jax import lax
from jax.experimental import pallas as pl
from jax.experimental.pallas import tpu as pltpu
from jax.sharding import PartitionSpec as P

TOPK = 2
LANES = 128
TILE = 16
N_X = 4
MESH = pl.DeviceIdType.MESH
F32 = jnp.float32
BF16 = jnp.bfloat16


def dot(a, b):
    return jnp.dot(a, b, preferred_element_type=F32)


def silu_mul(gate, up):
    return (gate / (1.0 + jnp.exp(-gate)) * up).astype(BF16)


def offset_at(place, reach, odd):
    groups = 2 * reach
    group, item = place // 4, lax.rem(place, 4)
    first = 1 - (group + groups - 2) // (groups - 1)
    later = group - 1 + first
    ring = first * reach * (1 - 2 * lax.rem(item, 2)) + (1 - first) * (
        (reach - 1 - later // 2) * (1 - 2 * lax.rem(later, 2))
    )
    return ring, first * (2 * (item // 2) + odd) + (1 - first) * item


def swapped(swap, read, blocks):
    stacked = jnp.concatenate([read(b) for b in range(blocks)], axis=0)
    return dot(swap, stacked).astype(BF16)


def order_matrix(outer, inner):
    side = outer * inner
    to = lax.broadcasted_iota(jnp.int32, (side, side), 0)
    come = lax.broadcasted_iota(jnp.int32, (side, side), 1)
    return jnp.where(come == lax.rem(to, inner) * outer + to // inner, 1.0, 0.0).astype(BF16)


def kernel(
    n_ep, n_tp, cap, chunk,
    tokens, routes, gates, pre_gain, w_gate, w_up, w_down, sh_gate, sh_up, sh_down, post_gain,
    out,
    normed, pick, swap, swap_out, swap_in, flat, half_flat, outgoing, arrived, results, returned,
    wg, wu, wd, wg2, wu2, wd2, xs, rs, all_gate, all_up, all_down, shared,
    out_blocks, out_landed, scales, scales_landed,
    w_sem, relay_send, relay_recv, send_sem, arrive_sem, back_send, back_recv,
    ring_send, ring_recv, pair_send, pair_recv,
    out_send, out_recv, scale_send, scale_recv,
):
    me, tp = lax.axis_index("ep"), lax.axis_index("tp")
    core, row = lax.rem(tp, 2), tp // 2
    n_row = n_tp // 2
    n_z = n_ep // N_X
    reach = n_z // 4
    z, x = me // N_X, lax.rem(me, N_X)
    rows, width = tokens.shape
    slots = n_ep * cap
    places = n_ep // 2
    n_chunks = places // chunk
    span = chunk * cap
    own = places - 4
    blocks = width // LANES
    half_blocks = blocks // 2
    half_cap = cap // 2
    other = lax.rem(me + n_ep // 2, n_ep)
    pair = tp + 1 - 2 * core

    def partner(place, odd, sign):
        ring, side = offset_at(place, reach, odd)
        return lax.rem(z + n_z + sign * ring, n_z), lax.rem(x + N_X + sign * side, N_X)

    def remote(source, target, send, receive, device):
        return pltpu.make_async_remote_copy(
            src_ref=source, dst_ref=target, send_sem=send, recv_sem=receive,
            device_id=device, device_id_type=MESH,
        )

    barrier = pltpu.get_barrier_semaphore()

    def greet_ep(i, carry):
        device = (lax.rem(me + i, n_ep), tp)
        pl.semaphore_signal(barrier, inc=1, device_id=device, device_id_type=MESH)
        return carry

    def greet_tp(i, carry):
        device = (me, lax.rem(tp + i, n_tp))
        pl.semaphore_signal(barrier, inc=1, device_id=device, device_id_type=MESH)
        return carry

    lax.fori_loop(1, n_ep, greet_ep, 0)
    lax.fori_loop(1, n_tp, greet_tp, 0)

    weight_copies = [
        pltpu.make_async_copy(source, target, w_sem.at[i])
        for i, (source, target) in enumerate(((w_gate, wg), (w_up, wu), (w_down, wd)))
    ]
    for copy in weight_copies:
        copy.start()
    for copy in weight_copies:
        copy.wait()
    pl.semaphore_wait(barrier, n_ep - 1 + n_tp - 1)

    first_set = (wg, wu, wd)
    second_set = (wg2, wu2, wd2)
    shared_set = (all_gate, all_up, all_down)
    for mine, theirs in zip(first_set, second_set):
        remote(mine.at[tp], theirs.at[tp], relay_send, relay_recv, (other, tp)).start()

    ahead = n_row // 2
    behind = n_row - 1 - ahead
    up_row = 2 * lax.rem(row + 1, n_row) + core
    down_row = 2 * lax.rem(row + n_row - 1, n_row) + core

    def ring_step(k, whole, step, sources=None):
        three = whole[0].at[pl.ds(0, 3)]
        if 1 <= step <= ahead:
            remote(three, three, ring_send.at[k, 0], ring_recv.at[k, 0, step - 1], (me, tp)).wait_recv()
        if 1 <= step <= behind:
            remote(three, three, ring_send.at[k, 1], ring_recv.at[k, 1, step - 1], (me, tp)).wait_recv()
        from_below = 2 * lax.rem(row + n_row - step, n_row) + core
        from_above = 2 * lax.rem(row + step, n_row) + core
        for n, ref in enumerate(whole):
            source = sources[n] if sources is not None else ref.at[from_below]
            if step < ahead:
                remote(
                    source, ref.at[from_below], ring_send.at[k, 0], ring_recv.at[k, 0, step],
                    (me, up_row),
                ).start()
            if step < behind:
                source = sources[n] if sources is not None else ref.at[from_above]
                remote(
                    source, ref.at[from_above], ring_send.at[k, 1], ring_recv.at[k, 1, step],
                    (me, down_row),
                ).start()
        for n, ref in enumerate(whole):
            if step <= ahead:
                source = sources[n] if sources is not None else ref.at[from_below]
                remote(
                    source, ref.at[from_below], pair_send.at[k, n], pair_recv.at[k, n], (me, pair)
                ).start()
            if 1 <= step <= behind:
                remote(
                    ref.at[from_above], ref.at[from_above], pair_send.at[k, n], pair_recv.at[k, n],
                    (me, pair),
                ).start()

    def ring_end(k, whole):
        for n, ref in enumerate(whole):
            part = ref.at[pl.ds(0, n_row)]
            remote(part, part, pair_send.at[k, n], pair_recv.at[k, n], (me, tp)).wait()
        for way, count in ((0, ahead), (1, behind)):
            for n, ref in enumerate(whole):
                if count > 0 and n == 0:
                    part = ref.at[pl.ds(0, 3 * count)]
                    remote(
                        part, part, ring_send.at[k, way], ring_recv.at[k, way, 0], (me, tp)
                    ).wait_send()

    shared_parts = (sh_gate, sh_up, sh_down)
    ring_step(0, shared_set, 0, shared_parts)
    for part, whole in zip(shared_parts, shared_set):
        whole[tp] = part[...]

    def norm_rows(i, carry):
        at = pl.ds(pl.multiple_of(i * TILE, TILE), TILE)
        values = tokens[at, :].astype(F32)
        scale = lax.rsqrt(jnp.mean(values * values, axis=1, keepdims=True) + 1e-06)
        normed[at, :] = (values * scale * pre_gain[...]).astype(BF16)
        return carry

    lax.fori_loop(0, rows // TILE, norm_rows, 0)

    down_at = lax.broadcasted_iota(jnp.int32, (rows, rows), 0)
    across_at = lax.broadcasted_iota(jnp.int32, (rows, rows), 1)
    diagonal = down_at == across_at

    def column(values):
        return jnp.sum(jnp.where(diagonal, values, 0.0), axis=1, keepdims=True)

    expert = lax.broadcasted_iota(jnp.int32, (rows, LANES), 1).astype(F32)
    first = column(routes[0:1, :].astype(F32))
    second = column(routes[1:2, :].astype(F32))
    match0 = jnp.where(first == expert, 1.0, 0.0)
    match1 = jnp.where(second == expert, 1.0, 0.0)
    earlier = jnp.where(across_at < down_at, 1.0, 0.0).astype(BF16)
    before = dot(earlier, (match0 + match1).astype(BF16))
    place0 = first * cap + jnp.sum(before * match0, axis=1, keepdims=True)
    place1 = second * cap + jnp.sum(before * match1, axis=1, keepdims=True)
    slot = lax.broadcasted_iota(jnp.int32, (rows, slots), 1).astype(F32)
    pick0 = jnp.where(slot == place0, 1.0, 0.0)
    pick1 = jnp.where(slot == place1, 1.0, 0.0)
    pick[0:rows, :] = pick0.astype(BF16)
    pick[rows : 2 * rows, :] = pick1.astype(BF16)
    either = (pick0 + pick1).astype(BF16)
    swap[...] = order_matrix(TILE, TILE)
    swap_out[...] = order_matrix(TILE, half_blocks)
    swap_in[...] = order_matrix(half_blocks, TILE)

    wide = 2 * LANES
    for j in range(width // wide):
        columns = pl.ds(j * wide, wide)
        flat[:, columns] = lax.dot_general(
            either, normed[:, columns], (((0,), (0,)), ((), ())), preferred_element_type=F32
        ).astype(BF16)

    def pack(i, carry):
        at = pl.ds(pl.multiple_of(i * TILE, TILE), TILE)
        mixed = swapped(swap[...], lambda b: flat[at, pl.ds(b * LANES, LANES)], blocks)
        outgoing[at] = mixed.reshape(TILE, TILE, LANES)
        return carry

    lax.fori_loop(0, slots // TILE, pack, 0)

    def send_home(place, carry):
        to_z, to_x = partner(place, 0, 1)
        target = to_z * N_X + to_x

        @pl.when(place != own)
        def _():
            remote(
                outgoing.at[pl.ds(target * cap, cap)], arrived.at[pl.ds(place * cap, cap)],
                send_sem, arrive_sem.at[place // chunk], (target, tp),
            ).start()

        return carry

    def send_second(place, carry):
        to_z, to_x = partner(place, 1, 1)
        target = to_z * N_X + to_x
        served = lax.rem(target + n_ep // 2, n_ep)
        there = places + place

        @pl.when(place != own)
        def _():
            remote(
                outgoing.at[pl.ds(served * cap, cap)], arrived.at[pl.ds(there * cap, cap)],
                send_sem, arrive_sem.at[there // chunk], (target, tp),
            ).start()

        return carry

    lax.fori_loop(0, places, send_home, 0)
    lax.fori_loop(0, places, send_second, 0)
    arrived[pl.ds(own * cap, cap)] = outgoing[pl.ds(me * cap, cap)]
    arrived[pl.ds((places + own) * cap, cap)] = outgoing[pl.ds(other * cap, cap)]

    def expert_step(n, weights):
        gate_ref, up_ref, down_ref = weights
        base = n * span
        full = n * chunk // places * places + own < n * chunk or (
            n * chunk // places * places + own >= (n + 1) * chunk
        )
        awaited = arrived.at[pl.ds(base, span if full else span - cap)]
        remote(awaited, awaited, send_sem, arrive_sem.at[n], (me, tp)).wait_recv()
        for g in range(span // TILE):
            at = pl.ds(g * TILE, TILE)
            mixed = swapped(swap[...], lambda b, g=g: arrived[base + g * TILE + b], TILE)
            for b in range(blocks):
                xs[at, pl.ds(b * LANES, LANES)] = mixed[TILE * b : TILE * (b + 1), :]
        taken = xs[...]
        ff = gate_ref.shape[2]
        gate = dot(taken, gate_ref[...].reshape(width, ff))
        hidden = silu_mul(gate, dot(taken, up_ref[...].reshape(width, ff)))
        for j in range(width // 512):
            columns = pl.ds(j * 512, 512)
            rs[:, columns] = dot(hidden, down_ref[:, :, columns].reshape(ff, 512)).astype(BF16)
        for h in range(2):
            for g in range(span // TILE):
                at = pl.ds(g * TILE, TILE)
                mixed = swapped(
                    swap_out[...],
                    lambda b, at=at, h=h: rs[at, pl.ds((2 * b + h) * LANES, LANES)],
                    half_blocks,
                )
                results[h, pl.ds(base // 2 + g * half_blocks, half_blocks)] = mixed.reshape(
                    half_blocks, TILE, LANES
                )

    def send_back(half, start, stop, odd):
        base = odd * places
        served = other if odd else me

        def one(place, carry):
            to_z, to_x = partner(place, odd, -1)

            @pl.when(place != own)
            def _():
                remote(
                    results.at[half, pl.ds((base + place) * half_cap, half_cap)],
                    returned.at[half, pl.ds(served * half_cap, half_cap)],
                    back_send.at[half], back_recv.at[half], (to_z * N_X + to_x, tp),
                ).start()

            return carry

        lax.fori_loop(start, stop, one, 0)

    def keep_own(odd):
        served = other if odd else me
        for h in range(2):
            returned[h, pl.ds(served * half_cap, half_cap)] = results[
                h, pl.ds((odd * places + own) * half_cap, half_cap)
            ]

    early = max(ahead - 1, 1)
    for step in range(1, early):
        ring_step(0, shared_set, step)
    three = wg2.at[pl.ds(0, 3)]
    remote(three, three, relay_send, relay_recv, (me, tp)).wait_recv()
    ring_step(1, second_set, 0)
    for n in range(n_chunks):
        expert_step(n, first_set)
        send_back(0, n * chunk, (n + 1) * chunk, 0)
        if 1 + n < ahead:
            ring_step(1, second_set, 1 + n)
    keep_own(0)
    send_back(1, 0, places, 0)
    for step in range(1 + n_chunks, ahead):
        ring_step(1, second_set, step)
    for step in range(early, ahead):
        ring_step(0, shared_set, step)
    ring_step(1, second_set, ahead)
    ring_end(1, second_set)
    for n in range(n_chunks):
        expert_step(n_chunks + n, second_set)
        send_back(0, n * chunk, (n + 1) * chunk, 1)
    keep_own(1)
    send_back(1, 0, places, 1)

    ring_step(0, shared_set, ahead)
    ring_end(0, shared_set)
    sh_ff = sh_gate.shape[1]
    gate_sum = dot(normed[...], all_gate[...].reshape(width, sh_ff))
    up_sum = dot(normed[...], all_up[...].reshape(width, sh_ff))
    shared_hidden = silu_mul(gate_sum, up_sum)
    out_width = width // n_tp
    for t in range(0, n_tp, 2):
        both = jnp.concatenate([all_down[t], all_down[t + 1]], axis=1)
        shared[:, pl.ds(t * out_width, 2 * out_width)] = dot(shared_hidden, both).astype(BF16)

    weight0, weight1 = column(gates[0:1, :]), column(gates[1:2, :])
    squares = jnp.zeros((rows, LANES), F32)
    for h in range(2):
        rest = pl.ds(0, (n_ep - 2) * half_cap)
        remote(
            results.at[h, rest], returned.at[h, rest], back_send.at[h], back_recv.at[h], (me, tp)
        ).wait_recv()

        def unpack(i, carry, h=h):
            tile = i * half_blocks
            mixed = swapped(swap_in[...], lambda b: returned[h, tile + b], half_blocks)
            at = pl.ds(pl.multiple_of(i * TILE, TILE), TILE)
            for b in range(half_blocks):
                half_flat[at, pl.ds(b * LANES, LANES)] = mixed[TILE * b : TILE * (b + 1), :]
            return carry

        lax.fori_loop(0, slots // TILE, unpack, 0)
        for jj in range(half_blocks // 2):
            picked = dot(pick[...], half_flat[:, pl.ds(jj * wide, wide)])
            routed = (weight0 * picked[0:rows] + weight1 * picked[rows : 2 * rows]).astype(BF16)
            for b in range(2):
                block = 2 * (2 * jj + b) + h
                total = routed[:, b * LANES : (b + 1) * LANES].astype(F32) + shared[
                    :, pl.ds(block * LANES, LANES)
                ].astype(F32)
                squares += total * total
                per = out_width // LANES
                out_blocks[block // per, :, pl.ds(block % per * LANES, LANES)] = total.astype(BF16)
        if out_width == LANES:
            send_out(h, n_row, row, tp, me, remote, out_blocks, out_landed, out_send, out_recv)
    if out_width != LANES:
        for h in range(2):
            send_out(h, n_row, row, tp, me, remote, out_blocks, out_landed, out_send, out_recv)

    scale_out = lax.rsqrt(jnp.sum(squares, axis=1, keepdims=True) * (1.0 / width) + 1e-06)
    scale_line = jnp.sum(jnp.where(diagonal, scale_out, 0.0), axis=0, keepdims=True)
    scales[...] = jnp.broadcast_to(scale_line, scales.shape)

    def send_scale(i, carry):
        target = lax.rem(tp + i, n_tp)
        remote(scales, scales_landed.at[tp], scale_send, scale_recv, (me, target)).start()
        return carry

    lax.fori_loop(1, n_tp, send_scale, 0)
    out_landed[tp] = out_blocks[tp]
    scales_landed[tp] = scales[...]

    remote(three, three, relay_send, relay_recv, (me, tp)).wait_send()
    rest = pl.ds(0, (n_ep - 2) * cap)
    remote(outgoing.at[rest], arrived.at[rest], send_sem, arrive_sem.at[0], (me, tp)).wait_send()
    for h in range(2):
        rest = pl.ds(0, (n_ep - 2) * half_cap)
        remote(
            results.at[h, rest], returned.at[h, rest], back_send.at[h], back_recv.at[h], (me, tp)
        ).wait_send()
    others = pl.ds(0, n_tp - 1)
    some = scales_landed.at[others]
    remote(some, some, scale_send, scale_recv, (me, tp)).wait()
    some = out_landed.at[others]
    remote(some, some, out_send, out_recv, (me, tp)).wait()

    gain = post_gain[:, pl.ds(pl.multiple_of(tp * out_width, LANES), out_width)]

    def finish(t, carry):
        scale = column(scales_landed[t][0:1, :])
        out[t] = (out_landed[t].astype(F32) * scale * gain).astype(BF16)
        return carry

    lax.fori_loop(0, n_tp, finish, 0)


def send_out(h, n_row, row, tp, me, remote, out_blocks, out_landed, out_send, out_recv):
    def one(i, carry):
        target = 2 * lax.rem(row + i, n_row) + h

        @pl.when(target != tp)
        def _():
            remote(
                out_blocks.at[target], out_landed.at[tp], out_send, out_recv, (me, target)
            ).start()

        return carry

    lax.fori_loop(0, n_row, one, 0)


def per_device(
    tokens, routes, gates, pre_gain, w_gate, w_up, w_down, sh_gate, sh_up, sh_down, post_gain
):
    rows, width = tokens.shape
    n_ep, n_tp = lax.axis_size("ep"), lax.axis_size("tp")
    ff = w_gate.shape[2]
    cap = max(2, 4 * rows * TOPK // (3 * n_ep))
    chunk = 8
    slots = n_ep * cap
    n_row = n_tp // 2
    depth, sh_ff = sh_gate.shape
    out_width = width // n_tp
    half_blocks = width // LANES // 2
    vmem = pl.BlockSpec(memory_space=pltpu.VMEM)
    anywhere = pl.BlockSpec(memory_space=pl.ANY)
    dma = pltpu.SemaphoreType.DMA
    tiles = pltpu.VMEM((slots, TILE, LANES), BF16)
    halves = pltpu.VMEM((2, slots // 2, TILE, LANES), BF16)
    in_rows = pltpu.VMEM((n_tp, width // n_tp, ff), BF16)
    out_rows = pltpu.VMEM((n_tp, ff // n_tp, width), BF16)
    result = pl.pallas_call(
        functools.partial(kernel, n_ep, n_tp, cap, chunk),
        out_shape=jax.ShapeDtypeStruct((n_tp, rows, out_width), BF16),
        in_specs=[vmem] * 4 + [anywhere] * 3 + [vmem] * 4,
        out_specs=vmem,
        scratch_shapes=[
            pltpu.VMEM((rows, width), BF16),
            pltpu.VMEM((2 * rows, slots), BF16),
            pltpu.VMEM((TILE * TILE, TILE * TILE), BF16),
            pltpu.VMEM((TILE * half_blocks, TILE * half_blocks), BF16),
            pltpu.VMEM((TILE * half_blocks, TILE * half_blocks), BF16),
            pltpu.VMEM((slots, width), BF16),
            pltpu.VMEM((slots, width // 2), BF16),
            tiles, tiles, halves, halves,
            in_rows, in_rows, out_rows, in_rows, in_rows, out_rows,
            pltpu.VMEM((chunk * cap, width), BF16),
            pltpu.VMEM((chunk * cap, width), BF16),
            pltpu.VMEM((n_tp, depth, sh_ff), BF16),
            pltpu.VMEM((n_tp, depth, sh_ff), BF16),
            pltpu.VMEM((n_tp, sh_ff, out_width), BF16),
            pltpu.VMEM((rows, width), BF16),
            pltpu.VMEM((n_tp, rows, out_width), BF16),
            pltpu.VMEM((n_tp, rows, out_width), BF16),
            pltpu.VMEM((8, rows), F32),
            pltpu.VMEM((n_tp, 8, rows), F32),
            dma((3,)), dma, dma, dma, dma((n_ep // chunk,)), dma((2,)), dma((2,)),
            dma((2, 2)), dma((2, 2, n_row // 2)), dma((2, 3)), dma((2, 3)),
            dma, dma, dma, dma,
        ],
        compiler_params=pltpu.CompilerParams(
            collective_id=0, has_side_effects=True, vmem_limit_bytes=60 * 1024 * 1024
        ),
    )(
        tokens, routes.T, gates.T, pre_gain.reshape(1, width),
        w_gate.reshape(n_tp, width // n_tp, ff), w_up.reshape(n_tp, width // n_tp, ff),
        w_down.reshape(n_tp, ff // n_tp, width),
        sh_gate, sh_up, sh_down, post_gain.reshape(1, width),
    )
    return result.reshape(n_tp * rows, out_width)


def solution(mesh):
    return jax.shard_map(
        per_device,
        mesh=mesh,
        in_specs=(
            P(("ep", "tp"), None),
            P(("ep", "tp"), None),
            P(("ep", "tp"), None),
            P(),
            P("ep", None, None),
            P("ep", None, None),
            P("ep", None, None),
            P("tp", None),
            P("tp", None),
            P(None, "tp"),
            P(),
        ),
        out_specs=P("ep", "tp"),
        check_vma=False,
    )
```

time: 354 us -> 146 us (0.41)
  waiting for transfers between devices: 207 us -> 0 us
  Pallas kernels: 0 us -> 144 us
  blocking collectives: 37.2 us -> 0 us
  local copies, waits for them, and re-layouts: 38.5 us -> 2.06 us
  starting transfers between devices: 26.1 us -> 0 us
  matrix products: 17.2 us -> 0 us
  other arithmetic: 13.6 us -> 0 us
  between operations: 13.3 us -> 0.01 us
    all_to_all x2 -> x0, waiting for transfers between devices: 205 us -> none  [the longest x1 106 us: per_device(): lax.all_to_all(outgoing, 'ep', split_axis=0, concat_axis=0, tiled=True)]
    pallas_call x0 -> x1, Pallas kernels: none -> 144 us  [per_device(): pl.pallas_call(functools.partial(kernel, n_ep, n_tp, cap, chunk), out_sha...]
    all_to_all x1 -> x0, blocking collectives: 37.2 us -> none  [per_device(): lax.all_to_all(out_rows, 'tp', split_axis=1, concat_axis=0, tiled=True)]
    all_to_all x2 -> x0, starting transfers between devices: 25.8 us -> none  [the longest x1 19 us: per_device(): lax.all_to_all(outgoing, 'ep', split_axis=0, concat_axis=0, tiled=True)]
    dot_general x4 -> x0, matrix products: 17.2 us -> none  [the longest x1 6 us: per_device(): jnp.dot(hidden, w_down[0], preferred_element_type=jnp.float32)]
    reshape x4 -> x0, local copies, waits for them, and re-layouts: 17 us -> none  [the longest x1 4.3 us: per_device(): picked = returned.reshape(experts_all * capacity, full_width)[dest_slot]]
    gather x2 -> x0, local copies, waits for them, and re-layouts: 10.1 us -> none  [the longest x1 6.85 us: per_device(): picked = returned.reshape(experts_all * capacity, full_width)[dest_slot]]
    reduce_sum x3 -> x0, other arithmetic: 9.23 us -> none  [the longest x1 7.76 us: per_device(): jnp.sum(weighted.reshape(tok_rows, TOPK, full_width), axis=1)]
  transfers between devices with their start and end apart: 5 -> 0, of which waited for: 2 -> 0; matrix products, arithmetic and copies ran while one was open for 13% -> 0% of each run, Pallas kernels for 0% -> 0%
where the time goes in v3:
time: 146 us
  Pallas kernels  144 us (99%)
  local copies, waits for them, and re-layouts  2.06 us (1%)
    pallas_call x1, Pallas kernels, per_device(): pl.pallas_call(functools.partial(kernel, n_ep, n_tp, cap, chunk), out_sha...  144 us

profile of v3, /device:TPU:1, one launch (start us, length us, event | category | flops | bytes accessed | tf_op | source)
XLA Modules:
  0.0 146.2 jit_solution(15756995460300652504)
XLA Ops:
  0.0 144.1 %shard_map.109 = bf16[16,192,128]{2,1,0:T(8,128)(2,1)} custom-call(bf16[192,2048]{1,0:T(8,128)(2,1)} %tokens.1, s32[2,192]{1,0:T(2,128)} %bitcast.14, f32[2,192]{1,0:T(2,128)} %bitcast.15, f32[1,2048]{1,0:T(1,128)} %bitcast.12, bf16[16,128,512]{2,1,0:T(8,128)(2,1)} %bitcast.9, bf16[16,128,512]{2,1,0:T(8,128)(2,1)} %bitcast.10, ...), custom_call_target="tpu_custom_call" | custom-call | tf_op jit(solution)/shard_map/pallas_call | solution.py:458
  144.1 2.1 %copy.13 = bf16[3072,128]{1,0:T(8,128)(2,1)} copy(bf16[3072,128]{1,0:T(8,128)(2,1)} %bitcast.8) | data formatting | bytes 1572864

commit v4 on v3

--- a/solution.py
+++ b/solution.py
@@ -49,12 +49,13 @@
 
 def kernel(
     n_ep, n_tp, cap, chunk,
-    tokens, routes, gates, pre_gain, w_gate, w_up, w_down, sh_gate, sh_up, sh_down, post_gain,
-    out,
+    tokens_in, routes_in, gates_in, pre_gain_in, w_gate, w_up, w_down, sh_gate, sh_up, sh_down,
+    out_landed, scales_landed,
+    tokens, routes, gates, pre_gain, slice_gate, slice_up, slice_down,
     normed, pick, swap, swap_out, swap_in, flat, half_flat, outgoing, arrived, results, returned,
     wg, wu, wd, wg2, wu2, wd2, xs, rs, all_gate, all_up, all_down, shared,
-    out_blocks, out_landed, scales, scales_landed,
-    w_sem, relay_send, relay_recv, send_sem, arrive_sem, back_send, back_recv,
+    out_blocks, scales,
+    in_sem, w_sem, relay_send, relay_recv, send_sem, arrive_sem, back_send, back_recv,
     ring_send, ring_recv, pair_send, pair_recv,
     out_send, out_recv, scale_send, scale_recv,
 ):
@@ -66,6 +67,7 @@
     z, x = me // N_X, lax.rem(me, N_X)
     rows, width = tokens.shape
     slots = n_ep * cap
+    unroll = next(u for u in (5, 4, 3, 2, 1) if slots // TILE % u == 0)
     places = n_ep // 2
     n_chunks = places // chunk
     span = chunk * cap
@@ -98,31 +100,40 @@
         pl.semaphore_signal(barrier, inc=1, device_id=device, device_id_type=MESH)
         return carry
 
+    first_set = (wg, wu, wd)
+    second_set = (wg2, wu2, wd2)
+    shared_set = (all_gate, all_up, all_down)
+    slices = (slice_gate, slice_up, slice_down)
+    loads = [
+        pltpu.make_async_copy(source, target, in_sem.at[i])
+        for i, (source, target) in enumerate(
+            (
+                (tokens_in, tokens), (pre_gain_in, pre_gain), (routes_in, routes),
+                (gates_in, gates),
+                (w_gate.at[tp], slice_gate), (w_up.at[tp], slice_up), (w_down.at[tp], slice_down),
+                (sh_gate, all_gate.at[tp]), (sh_up, all_up.at[tp]), (sh_down, all_down.at[tp]),
+            )
+        )
+    ]
+    for copy in loads:
+        copy.start()
     lax.fori_loop(1, n_ep, greet_ep, 0)
     lax.fori_loop(1, n_tp, greet_tp, 0)
-
     weight_copies = [
         pltpu.make_async_copy(source, target, w_sem.at[i])
-        for i, (source, target) in enumerate(((w_gate, wg), (w_up, wu), (w_down, wd)))
+        for i, (source, target) in enumerate(zip((w_gate, w_up, w_down), first_set))
     ]
     for copy in weight_copies:
         copy.start()
-    for copy in weight_copies:
+    for copy in loads[:4]:
         copy.wait()
-    pl.semaphore_wait(barrier, n_ep - 1 + n_tp - 1)
-
-    first_set = (wg, wu, wd)
-    second_set = (wg2, wu2, wd2)
-    shared_set = (all_gate, all_up, all_down)
-    for mine, theirs in zip(first_set, second_set):
-        remote(mine.at[tp], theirs.at[tp], relay_send, relay_recv, (other, tp)).start()
 
     ahead = n_row // 2
     behind = n_row - 1 - ahead
     up_row = 2 * lax.rem(row + 1, n_row) + core
     down_row = 2 * lax.rem(row + n_row - 1, n_row) + core
 
-    def ring_step(k, whole, step, sources=None):
+    def ring_step(k, whole, step):
         three = whole[0].at[pl.ds(0, 3)]
         if 1 <= step <= ahead:
             remote(three, three, ring_send.at[k, 0], ring_recv.at[k, 0, step - 1], (me, tp)).wait_recv()
@@ -131,21 +142,21 @@
         from_below = 2 * lax.rem(row + n_row - step, n_row) + core
         from_above = 2 * lax.rem(row + step, n_row) + core
         for n, ref in enumerate(whole):
-            source = sources[n] if sources is not None else ref.at[from_below]
+            source = ref.at[from_below]
             if step < ahead:
                 remote(
                     source, ref.at[from_below], ring_send.at[k, 0], ring_recv.at[k, 0, step],
                     (me, up_row),
                 ).start()
             if step < behind:
-                source = sources[n] if sources is not None else ref.at[from_above]
+                source = ref.at[from_above]
                 remote(
                     source, ref.at[from_above], ring_send.at[k, 1], ring_recv.at[k, 1, step],
                     (me, down_row),
                 ).start()
         for n, ref in enumerate(whole):
             if step <= ahead:
-                source = sources[n] if sources is not None else ref.at[from_below]
+                source = ref.at[from_below]
                 remote(
                     source, ref.at[from_below], pair_send.at[k, n], pair_recv.at[k, n], (me, pair)
                 ).start()
@@ -167,19 +178,14 @@
                         part, part, ring_send.at[k, way], ring_recv.at[k, way, 0], (me, tp)
                     ).wait_send()
 
-    shared_parts = (sh_gate, sh_up, sh_down)
-    ring_step(0, shared_set, 0, shared_parts)
-    for part, whole in zip(shared_parts, shared_set):
-        whole[tp] = part[...]
-
     def norm_rows(i, carry):
-        at = pl.ds(pl.multiple_of(i * TILE, TILE), TILE)
+        at = pl.ds(pl.multiple_of(i * 3 * TILE, TILE), 3 * TILE)
         values = tokens[at, :].astype(F32)
         scale = lax.rsqrt(jnp.mean(values * values, axis=1, keepdims=True) + 1e-06)
         normed[at, :] = (values * scale * pre_gain[...]).astype(BF16)
         return carry
 
-    lax.fori_loop(0, rows // TILE, norm_rows, 0)
+    lax.fori_loop(0, rows // (3 * TILE), norm_rows, 0)
 
     down_at = lax.broadcasted_iota(jnp.int32, (rows, rows), 0)
     across_at = lax.broadcasted_iota(jnp.int32, (rows, rows), 1)
@@ -203,6 +209,14 @@
     pick[0:rows, :] = pick0.astype(BF16)
     pick[rows : 2 * rows, :] = pick1.astype(BF16)
     either = (pick0 + pick1).astype(BF16)
+    for copy in loads[4:]:
+        copy.wait()
+    pl.semaphore_wait(barrier, n_ep - 1 + n_tp - 1)
+
+    for mine, theirs in zip(slices, second_set):
+        remote(mine, theirs.at[tp], relay_send, relay_recv, (other, tp)).start()
+    ring_step(0, shared_set, 0)
+
     swap[...] = order_matrix(TILE, TILE)
     swap_out[...] = order_matrix(TILE, half_blocks)
     swap_in[...] = order_matrix(half_blocks, TILE)
@@ -215,12 +229,15 @@
         ).astype(BF16)
 
     def pack(i, carry):
-        at = pl.ds(pl.multiple_of(i * TILE, TILE), TILE)
-        mixed = swapped(swap[...], lambda b: flat[at, pl.ds(b * LANES, LANES)], blocks)
-        outgoing[at] = mixed.reshape(TILE, TILE, LANES)
-        return carry
-
-    lax.fori_loop(0, slots // TILE, pack, 0)
+        for u in range(unroll):
+            at = pl.ds(pl.multiple_of((i * unroll + u) * TILE, TILE), TILE)
+            mixed = swapped(
+                swap[...], lambda b, at=at: flat[at, pl.ds(b * LANES, LANES)], blocks
+            )
+            outgoing[at] = mixed.reshape(TILE, TILE, LANES)
+        return carry
+
+    lax.fori_loop(0, slots // TILE // unroll, pack, 0)
 
     def send_home(place, carry):
         to_z, to_x = partner(place, 0, 1)
@@ -319,17 +336,19 @@
     three = wg2.at[pl.ds(0, 3)]
     remote(three, three, relay_send, relay_recv, (me, tp)).wait_recv()
     ring_step(1, second_set, 0)
+    for copy in weight_copies:
+        copy.wait()
     for n in range(n_chunks):
+        if 1 + n < ahead:
+            ring_step(1, second_set, 1 + n)
         expert_step(n, first_set)
         send_back(0, n * chunk, (n + 1) * chunk, 0)
-        if 1 + n < ahead:
-            ring_step(1, second_set, 1 + n)
-    keep_own(0)
-    send_back(1, 0, places, 0)
     for step in range(1 + n_chunks, ahead):
         ring_step(1, second_set, step)
     for step in range(early, ahead):
         ring_step(0, shared_set, step)
+    keep_own(0)
+    send_back(1, 0, places, 0)
     ring_step(1, second_set, ahead)
     ring_end(1, second_set)
     for n in range(n_chunks):
@@ -340,7 +359,7 @@
 
     ring_step(0, shared_set, ahead)
     ring_end(0, shared_set)
-    sh_ff = sh_gate.shape[1]
+    sh_ff = all_gate.shape[2]
     gate_sum = dot(normed[...], all_gate[...].reshape(width, sh_ff))
     up_sum = dot(normed[...], all_up[...].reshape(width, sh_ff))
     shared_hidden = silu_mul(gate_sum, up_sum)
@@ -358,14 +377,18 @@
         ).wait_recv()
 
         def unpack(i, carry, h=h):
-            tile = i * half_blocks
-            mixed = swapped(swap_in[...], lambda b: returned[h, tile + b], half_blocks)
-            at = pl.ds(pl.multiple_of(i * TILE, TILE), TILE)
-            for b in range(half_blocks):
-                half_flat[at, pl.ds(b * LANES, LANES)] = mixed[TILE * b : TILE * (b + 1), :]
+            for u in range(unroll):
+                group = i * unroll + u
+                tile = group * half_blocks
+                mixed = swapped(
+                    swap_in[...], lambda b, tile=tile: returned[h, tile + b], half_blocks
+                )
+                at = pl.ds(pl.multiple_of(group * TILE, TILE), TILE)
+                for b in range(half_blocks):
+                    half_flat[at, pl.ds(b * LANES, LANES)] = mixed[TILE * b : TILE * (b + 1), :]
             return carry
 
-        lax.fori_loop(0, slots // TILE, unpack, 0)
+        lax.fori_loop(0, slots // TILE // unroll, unpack, 0)
         for jj in range(half_blocks // 2):
             picked = dot(pick[...], half_flat[:, pl.ds(jj * wide, wide)])
             routed = (weight0 * picked[0:rows] + weight1 * picked[rows : 2 * rows]).astype(BF16)
@@ -410,14 +433,16 @@
     some = out_landed.at[others]
     remote(some, some, out_send, out_recv, (me, tp)).wait()
 
-    gain = post_gain[:, pl.ds(pl.multiple_of(tp * out_width, LANES), out_width)]
-
-    def finish(t, carry):
-        scale = column(scales_landed[t][0:1, :])
-        out[t] = (out_landed[t].astype(F32) * scale * gain).astype(BF16)
-        return carry
-
-    lax.fori_loop(0, n_tp, finish, 0)
+
+def finish(landed, scales, post_gain, out):
+    sources, rows, out_width = landed.shape
+    at = pl.multiple_of(lax.axis_index("tp") * out_width, LANES)
+    gain = post_gain[:, pl.ds(at, out_width)]
+    down_at = lax.broadcasted_iota(jnp.int32, (rows, rows), 0)
+    diagonal = down_at == lax.broadcasted_iota(jnp.int32, (rows, rows), 1)
+    for t in range(sources):
+        scale = jnp.sum(jnp.where(diagonal, scales[t, 0:1, :], 0.0), axis=1, keepdims=True)
+        out[t] = (landed[t].astype(F32) * scale * gain).astype(BF16)
 
 
 def send_out(h, n_row, row, tp, me, remote, out_blocks, out_landed, out_send, out_recv):
@@ -455,12 +480,22 @@
     halves = pltpu.VMEM((2, slots // 2, TILE, LANES), BF16)
     in_rows = pltpu.VMEM((n_tp, width // n_tp, ff), BF16)
     out_rows = pltpu.VMEM((n_tp, ff // n_tp, width), BF16)
-    result = pl.pallas_call(
+    landed, scales = pl.pallas_call(
         functools.partial(kernel, n_ep, n_tp, cap, chunk),
-        out_shape=jax.ShapeDtypeStruct((n_tp, rows, out_width), BF16),
-        in_specs=[vmem] * 4 + [anywhere] * 3 + [vmem] * 4,
-        out_specs=vmem,
+        out_shape=(
+            jax.ShapeDtypeStruct((n_tp, rows, out_width), BF16),
+            jax.ShapeDtypeStruct((n_tp, 8, rows), F32),
+        ),
+        in_specs=[anywhere] * 10,
+        out_specs=(vmem, vmem),
         scratch_shapes=[
+            pltpu.VMEM((rows, width), BF16),
+            pltpu.VMEM((2, rows), jnp.int32),
+            pltpu.VMEM((2, rows), F32),
+            pltpu.VMEM((1, width), F32),
+            pltpu.VMEM((width // n_tp, ff), BF16),
+            pltpu.VMEM((width // n_tp, ff), BF16),
+            pltpu.VMEM((ff // n_tp, width), BF16),
             pltpu.VMEM((rows, width), BF16),
             pltpu.VMEM((2 * rows, slots), BF16),
             pltpu.VMEM((TILE * TILE, TILE * TILE), BF16),
@@ -477,10 +512,8 @@
             pltpu.VMEM((n_tp, sh_ff, out_width), BF16),
             pltpu.VMEM((rows, width), BF16),
             pltpu.VMEM((n_tp, rows, out_width), BF16),
-            pltpu.VMEM((n_tp, rows, out_width), BF16),
             pltpu.VMEM((8, rows), F32),
-            pltpu.VMEM((n_tp, 8, rows), F32),
-            dma((3,)), dma, dma, dma, dma((n_ep // chunk,)), dma((2,)), dma((2,)),
+            dma((10,)), dma((3,)), dma, dma, dma, dma((n_ep // chunk,)), dma((2,)), dma((2,)),
             dma((2, 2)), dma((2, 2, n_row // 2)), dma((2, 3)), dma((2, 3)),
             dma, dma, dma, dma,
         ],
@@ -491,8 +524,20 @@
         tokens, routes.T, gates.T, pre_gain.reshape(1, width),
         w_gate.reshape(n_tp, width // n_tp, ff), w_up.reshape(n_tp, width // n_tp, ff),
         w_down.reshape(n_tp, ff // n_tp, width),
-        sh_gate, sh_up, sh_down, post_gain.reshape(1, width),
+        sh_gate, sh_up, sh_down,
     )
+    some = n_tp // 4
+    result = pl.pallas_call(
+        finish,
+        grid=(4,),
+        out_shape=jax.ShapeDtypeStruct((n_tp, rows, out_width), BF16),
+        in_specs=[
+            pl.BlockSpec((some, rows, out_width), lambda i: (i, 0, 0)),
+            pl.BlockSpec((some, 8, rows), lambda i: (i, 0, 0)),
+            pl.BlockSpec((1, width), lambda i: (0, 0)),
+        ],
+        out_specs=pl.BlockSpec((some, rows, out_width), lambda i: (i, 0, 0)),
+    )(landed, scales, post_gain.reshape(1, width))
     return result.reshape(n_tp * rows, out_width)
 
 

time: 146 us -> 142 us (0.973)
  Pallas kernels: 144 us -> 141 us
  local copies, waits for them, and re-layouts: 2.06 us -> 0 us
    pallas_call x1, Pallas kernels: 144 us -> 138 us  [per_device(): pl.pallas_call(functools.partial(kernel, n_ep, n_tp, cap, chunk), out_sha...]
    pallas_call x0 -> x1, Pallas kernels: none -> 3.62 us  [per_device(): pl.pallas_call(finish, grid=(4,), out_shape=jax.ShapeDtypeStruct((n_tp, r...]
    unnamed x1 -> x0, local copies, waits for them, and re-layouts: 2.06 us -> none
where the time goes in v4:
time: 142 us; the launch traced here: 141 us
  Pallas kernels  141 us (99%)
    pallas_call x1, Pallas kernels, per_device(): pl.pallas_call(functools.partial(kernel, n_ep, n_tp, cap, chunk), out_sha...  138 us
    pallas_call x1, Pallas kernels, per_device(): pl.pallas_call(finish, grid=(4,), out_shape=jax.ShapeDtypeStruct((n_tp, r...  3.62 us

profile of v4, /device:TPU:1, one launch (start us, length us, event | category | flops | bytes accessed | tf_op | source)
XLA Modules:
  0.0 141.5 jit_solution(9773021025234593108)
XLA Ops:
  0.0 137.8 %shard_map.109 = (bf16[16,192,128]{2,1,0:T(8,128)(2,1)}, f32[16,8,192]{2,1,0:T(8,128)}) custom-call(bf16[192,2048]{1,0:T(8,128)(2,1)} %tokens_in.1, s32[2,192]{1,0:T(2,128)} %bitcast.13, f32[2,192]{1,0:T(2,128)} %bitcast.14, f32[1,2048]{1,0:T(1,128)} %bitcast.12, bf16[16,128,512]{2,1,0:T(8,128)(2,1)} %bitcast.8, bf16[16,128,512]{2,1,0:T(8,128)(2,1)} %bitcast.9, ...), custom_call_target="tpu_custom_call" | custom-call | tf_op jit(solution)/shard_map/pallas_call | solution.py:483
  137.8 3.6 %shard_map.110 = bf16[16,192,128]{2,1,0:T(8,128)(2,1)} custom-call(bf16[16,192,128]{2,1,0:T(8,128)(2,1)} %get-tuple-element.7.landed, f32[16,8,192]{2,1,0:T(8,128)} %get-tuple-element.8.scales, f32[1,2048]{1,0:T(1,128)} %bitcast.11), custom_call_target="tpu_custom_call" | custom-call | tf_op jit(solution)/shard_map/pallas_call | solution.py:530

commit v5 on v4

--- a/solution.py
+++ b/solution.py
@@ -90,8 +90,12 @@
 
     barrier = pltpu.get_barrier_semaphore()
 
-    def greet_ep(i, carry):
-        device = (lax.rem(me + i, n_ep), tp)
+    near = (2 * reach + 1) * N_X
+    itself = reach * N_X
+
+    def greet_near(i, carry):
+        at_z = lax.rem(z + n_z + i // N_X - reach, n_z)
+        device = (at_z * N_X + lax.rem(x + lax.rem(i, N_X), N_X), tp)
         pl.semaphore_signal(barrier, inc=1, device_id=device, device_id_type=MESH)
         return carry
 
@@ -117,7 +121,9 @@
     ]
     for copy in loads:
         copy.start()
-    lax.fori_loop(1, n_ep, greet_ep, 0)
+    pl.semaphore_signal(barrier, inc=1, device_id=(other, tp), device_id_type=MESH)
+    lax.fori_loop(0, itself, greet_near, 0)
+    lax.fori_loop(itself + 1, near, greet_near, 0)
     lax.fori_loop(1, n_tp, greet_tp, 0)
     weight_copies = [
         pltpu.make_async_copy(source, target, w_sem.at[i])
@@ -133,50 +139,32 @@
     up_row = 2 * lax.rem(row + 1, n_row) + core
     down_row = 2 * lax.rem(row + n_row - 1, n_row) + core
 
-    def ring_step(k, whole, step):
-        three = whole[0].at[pl.ds(0, 3)]
-        if 1 <= step <= ahead:
-            remote(three, three, ring_send.at[k, 0], ring_recv.at[k, 0, step - 1], (me, tp)).wait_recv()
-        if 1 <= step <= behind:
-            remote(three, three, ring_send.at[k, 1], ring_recv.at[k, 1, step - 1], (me, tp)).wait_recv()
-        from_below = 2 * lax.rem(row + n_row - step, n_row) + core
-        from_above = 2 * lax.rem(row + step, n_row) + core
-        for n, ref in enumerate(whole):
-            source = ref.at[from_below]
-            if step < ahead:
-                remote(
-                    source, ref.at[from_below], ring_send.at[k, 0], ring_recv.at[k, 0, step],
-                    (me, up_row),
-                ).start()
-            if step < behind:
-                source = ref.at[from_above]
-                remote(
-                    source, ref.at[from_above], ring_send.at[k, 1], ring_recv.at[k, 1, step],
-                    (me, down_row),
-                ).start()
-        for n, ref in enumerate(whole):
-            if step <= ahead:
-                source = ref.at[from_below]
-                remote(
-                    source, ref.at[from_below], pair_send.at[k, n], pair_recv.at[k, n], (me, pair)
-                ).start()
-            if 1 <= step <= behind:
-                remote(
-                    ref.at[from_above], ref.at[from_above], pair_send.at[k, n], pair_recv.at[k, n],
-                    (me, pair),
-                ).start()
+    def ring_step(k, whole, n, step):
+        ref = whole[n]
+        ups, downs = (ahead, behind) if n < 2 else (behind, ahead)
+        below = ref.at[2 * lax.rem(row + n_row - step, n_row) + core]
+        above = ref.at[2 * lax.rem(row + step, n_row) + core]
+        ways = ((0, below, ups, up_row), (1, above, downs, down_row))
+        for way, block, hops, _ in ways:
+            if 1 <= step <= hops:
+                receive = ring_recv.at[3 * k + n, way, step - 1]
+                remote(block, block, ring_send.at[k, way], receive, (me, tp)).wait_recv()
+        for way, block, hops, target in ways:
+            if step < hops:
+                receive = ring_recv.at[3 * k + n, way, step]
+                remote(block, block, ring_send.at[k, way], receive, (me, target)).start()
+        for way, block, hops, _ in ways:
+            if way <= step <= hops:
+                remote(block, block, pair_send.at[k, n], pair_recv.at[k, n], (me, pair)).start()
 
     def ring_end(k, whole):
         for n, ref in enumerate(whole):
             part = ref.at[pl.ds(0, n_row)]
             remote(part, part, pair_send.at[k, n], pair_recv.at[k, n], (me, tp)).wait()
-        for way, count in ((0, ahead), (1, behind)):
-            for n, ref in enumerate(whole):
-                if count > 0 and n == 0:
-                    part = ref.at[pl.ds(0, 3 * count)]
-                    remote(
-                        part, part, ring_send.at[k, way], ring_recv.at[k, way, 0], (me, tp)
-                    ).wait_send()
+        for way, count in ((0, 2 * ahead + behind), (1, 2 * behind + ahead)):
+            part = whole[0].at[pl.ds(0, count)]
+            receive = ring_recv.at[3 * k, way, 0]
+            remote(part, part, ring_send.at[k, way], receive, (me, tp)).wait_send()
 
     def norm_rows(i, carry):
         at = pl.ds(pl.multiple_of(i * 3 * TILE, TILE), 3 * TILE)
@@ -211,11 +199,13 @@
     either = (pick0 + pick1).astype(BF16)
     for copy in loads[4:]:
         copy.wait()
-    pl.semaphore_wait(barrier, n_ep - 1 + n_tp - 1)
-
-    for mine, theirs in zip(slices, second_set):
-        remote(mine, theirs.at[tp], relay_send, relay_recv, (other, tp)).start()
-    ring_step(0, shared_set, 0)
+    pl.semaphore_wait(barrier, near + n_tp - 1)
+
+    for n in range(3):
+        target = second_set[n].at[tp]
+        remote(slices[n], target, relay_send, relay_recv.at[n], (other, tp)).start()
+    for n in range(3):
+        ring_step(0, shared_set, n, 0)
 
     swap[...] = order_matrix(TILE, TILE)
     swap_out[...] = order_matrix(TILE, half_blocks)
@@ -267,8 +257,8 @@
 
         return carry
 
-    lax.fori_loop(0, places, send_home, 0)
-    lax.fori_loop(0, places, send_second, 0)
+    lax.fori_loop(own + 1, places, send_home, 0)
+    lax.fori_loop(own + 1, places, send_second, 0)
     arrived[pl.ds(own * cap, cap)] = outgoing[pl.ds(me * cap, cap)]
     arrived[pl.ds((places + own) * cap, cap)] = outgoing[pl.ds(other * cap, cap)]
 
@@ -330,34 +320,35 @@
                 h, pl.ds((odd * places + own) * half_cap, half_cap)
             ]
 
-    early = max(ahead - 1, 1)
-    for step in range(1, early):
-        ring_step(0, shared_set, step)
-    three = wg2.at[pl.ds(0, 3)]
-    remote(three, three, relay_send, relay_recv, (me, tp)).wait_recv()
-    ring_step(1, second_set, 0)
+    order = sorted((2 * n + step, n, step) for n in range(3) for step in range(ahead + 1))
+    for _, n, step in order:
+        if step == 0:
+            block = second_set[n].at[tp]
+            remote(block, block, relay_send, relay_recv.at[n], (me, tp)).wait_recv()
+        ring_step(1, second_set, n, step)
+        if (n, step) == (2, 0):
+            lax.fori_loop(0, own, send_home, 0)
+            lax.fori_loop(0, own, send_second, 0)
+
     for copy in weight_copies:
         copy.wait()
-    for n in range(n_chunks):
-        if 1 + n < ahead:
-            ring_step(1, second_set, 1 + n)
-        expert_step(n, first_set)
-        send_back(0, n * chunk, (n + 1) * chunk, 0)
-    for step in range(1 + n_chunks, ahead):
-        ring_step(1, second_set, step)
-    for step in range(early, ahead):
-        ring_step(0, shared_set, step)
-    keep_own(0)
+    for n in range(2 * n_chunks):
+        if n == n_chunks:
+            keep_own(0)
+            ring_end(1, second_set)
+        if n % 2 == 0 and 1 + n // 2 < ahead:
+            for part in range(3):
+                ring_step(0, shared_set, part, 1 + n // 2)
+        expert_step(n, first_set if n < n_chunks else second_set)
+        odd = n // n_chunks
+        begin = n % n_chunks * chunk
+        send_back(0, begin, begin + chunk, odd)
+    keep_own(1)
     send_back(1, 0, places, 0)
-    ring_step(1, second_set, ahead)
-    ring_end(1, second_set)
-    for n in range(n_chunks):
-        expert_step(n_chunks + n, second_set)
-        send_back(0, n * chunk, (n + 1) * chunk, 1)
-    keep_own(1)
     send_back(1, 0, places, 1)
 
-    ring_step(0, shared_set, ahead)
+    for n in range(3):
+        ring_step(0, shared_set, n, ahead)
     ring_end(0, shared_set)
     sh_ff = all_gate.shape[2]
     gate_sum = dot(normed[...], all_gate[...].reshape(width, sh_ff))
@@ -419,7 +410,8 @@
     out_landed[tp] = out_blocks[tp]
     scales_landed[tp] = scales[...]
 
-    remote(three, three, relay_send, relay_recv, (me, tp)).wait_send()
+    three = wg2.at[pl.ds(0, 3)]
+    remote(three, three, relay_send, relay_recv.at[0], (me, tp)).wait_send()
     rest = pl.ds(0, (n_ep - 2) * cap)
     remote(outgoing.at[rest], arrived.at[rest], send_sem, arrive_sem.at[0], (me, tp)).wait_send()
     for h in range(2):
@@ -513,8 +505,8 @@
             pltpu.VMEM((rows, width), BF16),
             pltpu.VMEM((n_tp, rows, out_width), BF16),
             pltpu.VMEM((8, rows), F32),
-            dma((10,)), dma((3,)), dma, dma, dma, dma((n_ep // chunk,)), dma((2,)), dma((2,)),
-            dma((2, 2)), dma((2, 2, n_row // 2)), dma((2, 3)), dma((2, 3)),
+            dma((10,)), dma((3,)), dma, dma((3,)), dma, dma((n_ep // chunk,)), dma((2,)), dma((2,)),
+            dma((2, 2)), dma((6, 2, n_row // 2)), dma((2, 3)), dma((2, 3)),
             dma, dma, dma, dma,
         ],
         compiler_params=pltpu.CompilerParams(

time: 142 us -> 146 us (1.028)
  Pallas kernels: 141 us -> 145 us
    pallas_call x1, Pallas kernels: 138 us -> 142 us  [per_device(): pl.pallas_call(functools.partial(kernel, n_ep, n_tp, cap, chunk), out_sha...]
where the time goes in v5:
time: 146 us; the launch traced here: 145 us
  Pallas kernels  145 us (99%)
    pallas_call x1, Pallas kernels, per_device(): pl.pallas_call(functools.partial(kernel, n_ep, n_tp, cap, chunk), out_sha...  142 us
    pallas_call x1, Pallas kernels, per_device(): pl.pallas_call(finish, grid=(4,), out_shape=jax.ShapeDtypeStruct((n_tp, r...  3.62 us

profile of v5, /device:TPU:1, one launch (start us, length us, event | category | flops | bytes accessed | tf_op | source)
XLA Modules:
  0.0 145.4 jit_solution(7380736614271040473)
XLA Ops:
  0.0 141.8 %shard_map.109 = (bf16[16,192,128]{2,1,0:T(8,128)(2,1)}, f32[16,8,192]{2,1,0:T(8,128)}) custom-call(bf16[192,2048]{1,0:T(8,128)(2,1)} %tokens_in.1, s32[2,192]{1,0:T(2,128)} %bitcast.13, f32[2,192]{1,0:T(2,128)} %bitcast.14, f32[1,2048]{1,0:T(1,128)} %bitcast.12, bf16[16,128,512]{2,1,0:T(8,128)(2,1)} %bitcast.8, bf16[16,128,512]{2,1,0:T(8,128)(2,1)} %bitcast.9, ...), custom_call_target="tpu_custom_call" | custom-call | tf_op jit(solution)/shard_map/pallas_call | solution.py:475
  141.8 3.6 %shard_map.110 = bf16[16,192,128]{2,1,0:T(8,128)(2,1)} custom-call(bf16[16,192,128]{2,1,0:T(8,128)(2,1)} %get-tuple-element.7.landed, f32[16,8,192]{2,1,0:T(8,128)} %get-tuple-element.8.scales, f32[1,2048]{1,0:T(1,128)} %bitcast.11), custom_call_target="tpu_custom_call" | custom-call | tf_op jit(solution)/shard_map/pallas_call | solution.py:522

commit v6 on v5

--- a/solution.py
+++ b/solution.py
@@ -257,8 +257,8 @@
 
         return carry
 
-    lax.fori_loop(own + 1, places, send_home, 0)
-    lax.fori_loop(own + 1, places, send_second, 0)
+    lax.fori_loop(0, places, send_home, 0)
+    lax.fori_loop(0, places, send_second, 0)
     arrived[pl.ds(own * cap, cap)] = outgoing[pl.ds(me * cap, cap)]
     arrived[pl.ds((places + own) * cap, cap)] = outgoing[pl.ds(other * cap, cap)]
 
@@ -320,15 +320,16 @@
                 h, pl.ds((odd * places + own) * half_cap, half_cap)
             ]
 
+    between = {(0, 0): 1, (1, 3): 2}
     order = sorted((2 * n + step, n, step) for n in range(3) for step in range(ahead + 1))
     for _, n, step in order:
         if step == 0:
             block = second_set[n].at[tp]
             remote(block, block, relay_send, relay_recv.at[n], (me, tp)).wait_recv()
         ring_step(1, second_set, n, step)
-        if (n, step) == (2, 0):
-            lax.fori_loop(0, own, send_home, 0)
-            lax.fori_loop(0, own, send_second, 0)
+        if (n, step) in between and between[n, step] < ahead:
+            for part in range(3):
+                ring_step(0, shared_set, part, between[n, step])
 
     for copy in weight_copies:
         copy.wait()
@@ -336,15 +337,16 @@
         if n == n_chunks:
             keep_own(0)
             ring_end(1, second_set)
-        if n % 2 == 0 and 1 + n // 2 < ahead:
+        if n == 2 and ahead > 3:
             for part in range(3):
-                ring_step(0, shared_set, part, 1 + n // 2)
+                ring_step(0, shared_set, part, 3)
         expert_step(n, first_set if n < n_chunks else second_set)
         odd = n // n_chunks
         begin = n % n_chunks * chunk
         send_back(0, begin, begin + chunk, odd)
+        if n == n_chunks:
+            send_back(1, 0, places, 0)
     keep_own(1)
-    send_back(1, 0, places, 0)
     send_back(1, 0, places, 1)
 
     for n in range(3):

time: 146 us -> 154 us (1.055)
  Pallas kernels: 145 us -> 154 us
    pallas_call x1, Pallas kernels: 142 us -> 151 us  [per_device(): pl.pallas_call(functools.partial(kernel, n_ep, n_tp, cap, chunk), out_sha...]
where the time goes in v6:
time: 154 us
  Pallas kernels  154 us (100%)
    pallas_call x1, Pallas kernels, per_device(): pl.pallas_call(functools.partial(kernel, n_ep, n_tp, cap, chunk), out_sha...  151 us
    pallas_call x1, Pallas kernels, per_device(): pl.pallas_call(finish, grid=(4,), out_shape=jax.ShapeDtypeStruct((n_tp, r...  3.62 us

profile of v6, /device:TPU:1, one launch (start us, length us, event | category | flops | bytes accessed | tf_op | source)
XLA Modules:
  0.0 154.3 jit_solution(10695625869378416972)
XLA Ops:
  0.0 150.6 %shard_map.109 = (bf16[16,192,128]{2,1,0:T(8,128)(2,1)}, f32[16,8,192]{2,1,0:T(8,128)}) custom-call(bf16[192,2048]{1,0:T(8,128)(2,1)} %tokens_in.1, s32[2,192]{1,0:T(2,128)} %bitcast.13, f32[2,192]{1,0:T(2,128)} %bitcast.14, f32[1,2048]{1,0:T(1,128)} %bitcast.12, bf16[16,128,512]{2,1,0:T(8,128)(2,1)} %bitcast.8, bf16[16,128,512]{2,1,0:T(8,128)(2,1)} %bitcast.9, ...), custom_call_target="tpu_custom_call" | custom-call | tf_op jit(solution)/shard_map/pallas_call | solution.py:477
  150.7 3.6 %shard_map.110 = bf16[16,192,128]{2,1,0:T(8,128)(2,1)} custom-call(bf16[16,192,128]{2,1,0:T(8,128)(2,1)} %get-tuple-element.7.landed, f32[16,8,192]{2,1,0:T(8,128)} %get-tuple-element.8.scales, f32[1,2048]{1,0:T(1,128)} %bitcast.11), custom_call_target="tpu_custom_call" | custom-call | tf_op jit(solution)/shard_map/pallas_call | solution.py:524
